TPU v7x, 128 devices: a whole 4x4x4 slice. The times are simulated.
128 devices in a mesh: sp: 32 (over z, y, core), tp: 4 (over x).
Axes of the slice: x: 4, y: 4, z: 4, core: 2. Of those that a mesh axis runs over, the one named last changes fastest.
Arguments:
- residual: bfloat16 [32768, 2048], P('sp'), may hold values from -6 to 6
- small_heads: bfloat16 [32768, 1024], P('sp', 'tp'), may hold values from -6 to 6
- large_heads: bfloat16 [32768, 1024], P('sp', 'tp'), may hold values from -6 to 6
- state_keys: bfloat16 [32768, 8, 128], P('sp', 'tp'), may hold values from -6 to 6
- state_queries: bfloat16 [32768, 8, 128], P('sp', 'tp'), may hold values from -6 to 6
- small_gate: bfloat16 [32768, 1024], P('sp', 'tp'), may hold values from -6 to 6
- large_gate: bfloat16 [32768, 1024], P('sp', 'tp'), may hold values from -6 to 6
- small_step: float32 [32768, 16], P('sp', 'tp'), may hold values from -3 to 2
- large_step: float32 [32768, 8], P('sp', 'tp'), may hold values from -3 to 2
- small_taps: bfloat16 [4, 1024], P(None, 'tp'), may hold values from -3 to 3
- large_taps: bfloat16 [4, 1024], P(None, 'tp'), may hold values from -3 to 3
- key_taps: bfloat16 [4, 8, 128], P(None, 'tp'), may hold values from -3 to 3
- query_taps: bfloat16 [4, 8, 128], P(None, 'tp'), may hold values from -3 to 3
- small_decay: float32 [16], P('tp'), may hold values from -12 to -2, as said below
- large_decay: float32 [8], P('tp'), may hold values from -12 to -2, as said below
- small_gain: bfloat16 [1024], P('tp'), may hold values from 0.099609375 to 1.8984375
- large_gain: bfloat16 [1024], P('tp'), may hold values from 0.099609375 to 1.8984375
- small_out: bfloat16 [1024, 2048], P('tp'), may hold values from -0.125 to 0.125
- large_out: bfloat16 [1024, 2048], P('tp'), may hold values from -0.125 to 0.125
- mixer_gain: bfloat16 [2048], replicated, may hold values from 0.099609375 to 1.8984375
- ffn_in_gain: bfloat16 [2048], replicated, may hold values from 0.099609375 to 1.8984375
- gate_proj: bfloat16 [2048, 5632], P('sp', 'tp'), may hold values from -0.125 to 0.125
- up_proj: bfloat16 [2048, 5632], P('sp', 'tp'), may hold values from -0.125 to 0.125
- down_proj: bfloat16 [2048, 5632], P('sp', 'tp'), may hold values from -0.078125 to 0.078125
- ffn_out_gain: bfloat16 [2048], replicated, may hold values from 0.099609375 to 1.8984375
Outputs:
- updated: bfloat16 [32768, 2048], P(('sp', 'tp'))
Inputs may be any that keep to these rules, and one draw needn't show every extreme that they name: `small_decay`: log decay rates of the first group. `large_decay`: log decay rates of the second group.
All inputs are finite; a program needn't handle non-finite values.
Results may differ from a plain program's by a relative error of at most 0.014.
Values may be sent and summed in bfloat16 or wider, within the bound.
A program may use at most 192 MiB of HBM per device.

v0:
```python
import jax
import jax.numpy as jnp
from jax import lax
from jax.sharding import Mesh
from jax.sharding import PartitionSpec as P

BLOCK = 128
SP = ("sp_0", "sp_1", "sp_2")
SP_TP = ("sp_0", "sp_1", "sp_2", "tp")


EPS = 1e-06


def passed_along(block, axis, distance):
    devices = range(lax.axis_size(axis))
    route = [(i - distance, i) for i in devices if i - distance in devices]
    return lax.ppermute(block, axis, route)


def nothing_yet(array, identity):
    return jax.tree.map(
        lambda a, e: jnp.broadcast_to(jnp.asarray(e, a.dtype), a.shape), array, identity
    )


def collected_together(array, axis):
    leaves = jax.tree.leaves(array)
    sequence = sorted(range(len(leaves)), key=lambda k: -leaves[k].size)
    width = (1, *leaves[sequence[0]].shape)[-1]
    lines = [
        jnp.pad(leaves[k].reshape(-1), (0, -leaves[k].size % width)).reshape(-1, width)
        for k in sequence
    ]
    both, at, found = (lax.all_gather(jnp.concatenate(lines), axis), 0, {})
    for k, line in zip(sequence, lines):
        slab = both[:, at : at + len(line)].reshape(len(both), -1)
        found[k] = slab[:, : leaves[k].size].reshape(-1, *leaves[k].shape)
        at += len(line)
    numbers = iter(range(len(leaves)))
    return jax.tree.map(lambda _: found[next(numbers)], array)


def prefix_by_axis(array, axes, combine, identity):
    before = start = nothing_yet(array, identity)
    subtotal = array
    for axis in reversed(axes):
        peers, position = (lax.axis_size(axis), lax.axis_index(axis))
        pieces = collected_together(
            jax.tree.map(
                lambda part, kind: part.astype(kind),
                subtotal,
                (jnp.bfloat16, jnp.bfloat16, jnp.bfloat16, jnp.bfloat16),
            ),
            axis,
        )
        inside, subtotal = (start, start)
        for k in range(peers):
            passed = k < position
            subtotal = combine(
                subtotal, jax.tree.map(lambda part, own: part[k].astype(own.dtype), pieces, array)
            )
            inside = jax.tree.map(lambda new, old: jnp.where(passed, new, old), subtotal, inside)
        before = combine(inside, before)
    return before


def in_one_piece(arrays, axis, dim, along):
    both = jnp.concatenate(arrays, axis=along)
    whole, at, finished = (lax.all_gather(both, axis, axis=dim, tiled=True), 0, [])
    for a in arrays:
        finished.append(lax.slice_in_dim(whole, at, at + a.shape[along], axis=along))
        at += a.shape[along]
    return tuple(finished)


def in_order(pieces, dim):
    pieces = jnp.moveaxis(pieces, 0, dim)
    dims = pieces.shape
    return pieces.reshape(*dims[:dim], dims[dim] * dims[dim + 1], *dims[dim + 2 :])


def all_blocks(array, axes, sequence):
    pieces = array
    for k in sequence:
        pieces = lax.all_gather(pieces, axes[k])
    done = sequence[::-1]
    back = [done.index(k) for k in range(len(axes))]
    pieces = pieces.transpose(*back, *range(len(axes), pieces.ndim))
    return pieces.reshape(-1, *array.shape)


def gather_axes(array, axes, sequence, dim):
    return in_order(all_blocks(array, axes, sequence), dim)


def causal_taps(extended, tap_weights, length):
    kernel_len = tap_weights.shape[0]
    summed = jnp.zeros((length,) + extended.shape[1:], jnp.float32)
    for offset in range(kernel_len):
        window_rows = extended[offset : offset + length].astype(jnp.float32)
        summed = summed + tap_weights[offset].astype(jnp.float32) * window_rows
    return jax.nn.silu(summed).astype(jnp.bfloat16)


def block_pass(values, key_rows, queries, step_sizes, decay_rates):
    length, groups, head_count, head_dim = values.shape
    block_count = length // BLOCK
    state_len = key_rows.shape[-1]
    log_decay = -step_sizes * decay_rates
    causal = jnp.tril(jnp.ones((BLOCK, BLOCK), dtype=bool))

    def one_block(carry_state, block):
        block_values, block_keys, block_queries, block_steps, block_decay = block
        cumulative = jnp.cumsum(block_decay, axis=0)
        scores = jnp.einsum(
            "lgn,sgn->gls", block_queries, block_keys, preferred_element_type=jnp.float32
        )
        cum_heads = jnp.transpose(cumulative, (1, 2, 0))
        gap_matrix = cum_heads[:, :, :, None] - cum_heads[:, :, None, :]
        decays = jnp.exp(jnp.where(causal, gap_matrix, -jnp.inf))
        step_heads = jnp.transpose(block_steps, (1, 2, 0))[:, :, None, :]
        weights = (scores[:, None] * decays * step_heads).astype(jnp.bfloat16)
        inside = jnp.einsum(
            "ghls,sghp->lghp", weights, block_values, preferred_element_type=jnp.float32
        )
        carried = jnp.einsum("lgn,ghpn->lghp", block_queries.astype(jnp.float32), carry_state)
        carried = carried * jnp.exp(cumulative)[..., None]
        tail_sum = cumulative[-1]
        scaled = (
            block_values.astype(jnp.float32)
            * (block_steps * jnp.exp(tail_sum - cumulative))[..., None]
        )
        fresh_state = jnp.einsum(
            "lghp,lgn->ghpn",
            scaled.astype(jnp.bfloat16),
            block_keys,
            preferred_element_type=jnp.float32,
        )
        next_state = carry_state * jnp.exp(tail_sum)[..., None, None] + fresh_state
        return (next_state, (inside + carried, cumulative))

    blocked = (
        values.reshape(block_count, BLOCK, groups, head_count, head_dim),
        key_rows.reshape(block_count, BLOCK, groups, state_len),
        queries.reshape(block_count, BLOCK, groups, state_len),
        step_sizes.reshape(block_count, BLOCK, groups, head_count),
        log_decay.reshape(block_count, BLOCK, groups, head_count),
    )
    start_state = jnp.zeros((groups, head_count, head_dim, state_len), jnp.float32)
    end_state, (outputs, cumulative) = lax.scan(one_block, start_state, blocked)
    tail_sums = cumulative[:, -1]
    offsets = jnp.cumsum(tail_sums, axis=0) - tail_sums
    device_cum = (cumulative + offsets[:, None]).reshape(length, groups, head_count)
    return (
        outputs.reshape(length, groups, head_count, head_dim),
        device_cum,
        end_state,
        jnp.sum(tail_sums, axis=0),
    )


def head_group(values, key_rows, queries, step_raw, decay_log):
    length = values.shape[0]
    head_count = step_raw.shape[1]
    groups = key_rows.shape[1]
    per_group = head_count // groups
    head_dim = values.shape[1] // head_count
    step_sizes = jax.nn.softplus(step_raw).reshape(length, groups, per_group)
    decay_rates = jnp.exp(decay_log).reshape(groups, per_group)
    return block_pass(
        values.reshape(length, groups, per_group, head_dim),
        key_rows,
        queries,
        step_sizes,
        decay_rates,
    )


def add_entering(outputs, queries, device_cum, entering):
    extra = jnp.einsum("lgn,ghpn->lghp", queries.astype(jnp.float32), entering)
    return outputs + extra * jnp.exp(device_cum)[..., None]


def unit_rms(values):
    return values * lax.rsqrt(jnp.mean(values * values, axis=-1, keepdims=True) + EPS)


def gate_and_norm(mixed_heads, gate_raw, gain):
    length, groups, per_group, head_dim = mixed_heads.shape
    gated = mixed_heads.reshape(length, -1) * jax.nn.silu(gate_raw.astype(jnp.float32))
    normed = unit_rms(gated.reshape(length, groups * per_group, head_dim))
    return (normed.reshape(length, -1) * gain.astype(jnp.float32)).astype(jnp.bfloat16)


def local(
    residual,
    small_heads,
    large_heads,
    state_keys,
    state_queries,
    small_gate,
    large_gate,
    small_step,
    large_step,
    small_taps,
    large_taps,
    key_taps,
    query_taps,
    small_decay,
    large_decay,
    small_gain,
    large_gain,
    small_out,
    large_out,
    mixer_gain,
    ffn_in_gain,
    gate_proj,
    up_proj,
    down_proj,
    ffn_out_gain,
):
    length = residual.shape[0]
    halo_rows = small_taps.shape[0] - 1
    first_row = length - halo_rows
    previous = passed_along(
        (
            small_heads[first_row:],
            large_heads[first_row:],
            state_keys[first_row:],
            state_queries[first_row:],
        ),
        SP,
        1,
    )
    small_conv = causal_taps(
        jnp.concatenate([previous[0], small_heads], axis=0), small_taps, length
    )
    large_conv = causal_taps(
        jnp.concatenate([previous[1], large_heads], axis=0), large_taps, length
    )
    key_conv = causal_taps(jnp.concatenate([previous[2], state_keys], axis=0), key_taps, length)
    query_conv = causal_taps(
        jnp.concatenate([previous[3], state_queries], axis=0), query_taps, length
    )
    small_out_local, small_cum, small_end, small_total = head_group(
        small_conv, key_conv[:, 0:1], query_conv[:, 0:1], small_step, small_decay
    )
    large_out_local, large_cum, large_end, large_total = head_group(
        large_conv, key_conv[:, 1:2], query_conv[:, 1:2], large_step, large_decay
    )

    def join(earlier, later):
        return (
            earlier[0] * jnp.exp(later[1])[..., None, None] + later[0],
            earlier[1] + later[1],
            earlier[2] * jnp.exp(later[3])[..., None, None] + later[2],
            earlier[3] + later[3],
        )

    identity_parts = (
        jnp.zeros_like(small_end),
        jnp.zeros_like(small_total),
        jnp.zeros_like(large_end),
        jnp.zeros_like(large_total),
    )
    entered = prefix_by_axis(
        (small_end, small_total, large_end, large_total), SP, join, identity_parts
    )
    small_enter = entered[0]
    large_enter = entered[2]
    small_mix = add_entering(small_out_local, query_conv[:, 0:1], small_cum, small_enter)
    large_mix = add_entering(large_out_local, query_conv[:, 1:2], large_cum, large_enter)
    small_normed = gate_and_norm(small_mix, small_gate, small_gain)
    large_normed = gate_and_norm(large_mix, large_gate, large_gain)
    partial_value = jnp.dot(small_normed, small_out, preferred_element_type=jnp.float32)
    partial_value = partial_value + jnp.dot(
        large_normed, large_out, preferred_element_type=jnp.float32
    )
    mix = lax.psum(partial_value.astype(jnp.bfloat16), "tp").astype(jnp.float32)
    mixed = residual.astype(jnp.float32) + unit_rms(mix) * mixer_gain.astype(jnp.float32)
    normed_in = (unit_rms(mixed) * ffn_in_gain.astype(jnp.float32)).astype(jnp.bfloat16)
    pieces = in_one_piece((gate_proj, up_proj), SP, 0, 1)
    gate = jnp.dot(normed_in, pieces[0], preferred_element_type=jnp.float32)
    up_values = jnp.dot(normed_in, pieces[1], preferred_element_type=jnp.float32)
    down_full = gather_axes(down_proj, (("sp_0", "sp_1"), "sp_2"), (0, 1), 0)
    hidden = (jax.nn.silu(gate) * up_values).astype(jnp.bfloat16)
    share = length // lax.axis_size("tp")
    ffn = lax.psum_scatter(
        lax.dot_general(
            hidden, down_full, (((1,), (1,)), ((), ())), preferred_element_type=jnp.float32
        ).astype(jnp.bfloat16),
        "tp",
        scatter_dimension=0,
        tiled=True,
    ).astype(jnp.float32)
    own_rows = lax.dynamic_slice_in_dim(mixed, lax.axis_index("tp") * share, share, 0)
    updated = own_rows + 0.5 * unit_rms(ffn) * ffn_out_gain.astype(jnp.float32)
    return updated.astype(jnp.bfloat16)


def solution(mesh):
    torus = Mesh(mesh.devices.reshape(4, 4, 2, mesh.shape["tp"]), ("sp_0", "sp_1", "sp_2", "tp"))
    in_specs = (
        P(SP, None),
        P(SP, "tp"),
        P(SP, "tp"),
        P(SP, "tp", None),
        P(SP, "tp", None),
        P(SP, "tp"),
        P(SP, "tp"),
        P(SP, "tp"),
        P(SP, "tp"),
        P(None, "tp"),
        P(None, "tp"),
        P(None, "tp", None),
        P(None, "tp", None),
        P("tp"),
        P("tp"),
        P("tp"),
        P("tp"),
        P("tp", None),
        P("tp", None),
        P(),
        P(),
        P(SP, "tp"),
        P(SP, "tp"),
        P(SP, "tp"),
        P(),
    )
    out_specs = P(SP_TP, None)
    return jax.shard_map(local, mesh=torus, in_specs=in_specs, out_specs=out_specs, check_vma=False)
```

profile of v0, /device:TPU:1, one launch (start us, length us, event | category | flops | bytes accessed | tf_op | source)
XLA Modules:
  0.0 482.5 jit_solution(811788357132697715)
XLA Ops:
  9.0 4.6 collective-permute-start
  13.6 1.1 copy.228
  14.7 1.9 collective-permute-start.1
  16.6 1.1 copy.231
  18.5 3.6 collective-permute-start.2
  23.0 1.9 collective-permute-start.3
  24.9 2.0 copy.226
  27.0 2.1 copy.240
  35.7 1.2 copy.248
  39.0 1.2 copy.253
  41.0 3.1 fusion.118
  45.9 2.5 multiply_convert_fusion.9
  49.2 83.8 %while.30 = (s32[]{:T(128)}, f32[1,4,64,128]{3,2,1,0:T(8,128)S(1)}, f32[8,128,1,4,64]{1,0,4,3,2:T(8,128)}, f32[8,128,1,4]{3,1,2,0:T(8,128)}, f32[8,128,1,4]{3,1,...) while((s32[]{:T(128)}, f32[1,4,64,128]{3,2,1,0:T(8,128)S(1)}, ...), condition=%wide.region_2.3_spmd.clone, body=%wide.region_0.2_spmd.clone.sunk | while | flops 30065156 | bytes 1596155 | solution.py:151
  53.5 1.1 fusion.250
  54.6 4.4 dynamic_update_slice.27
  64.0 1.1 fusion.250
  65.1 4.4 dynamic_update_slice.27
  74.4 1.1 fusion.250
  75.6 4.4 dynamic_update_slice.27
  84.9 1.1 fusion.250
  86.0 4.4 dynamic_update_slice.27
  95.4 1.1 fusion.250
  96.5 4.4 dynamic_update_slice.27
  105.9 1.1 fusion.250
  107.0 4.4 dynamic_update_slice.27
  116.3 1.1 fusion.250
  117.5 4.4 dynamic_update_slice.27
  126.8 1.1 fusion.250
  127.9 4.4 dynamic_update_slice.27
  134.7 3.0 fusion.119
  138.7 86.1 %while.31 = (s32[]{:T(128)}, f32[1,2,128,128]{3,2,1,0:T(8,128)S(1)}, f32[8,128,1,2,128]{1,0,4,3,2:T(8,128)}, f32[8,128,1,2]{3,1,2,0:T(8,128)}, f32[8,128,1,2]{3,...) while((s32[]{:T(128)}, ...), condition=%wide.region_5.6_spmd.clone, body=%wide.region_3.5_spmd.clone.sunk | while | flops 29868292 | bytes 1569483 | solution.py:151
  143.0 1.1 fusion.266
  144.1 4.8 dynamic_update_slice.29
  153.8 1.1 fusion.266
  154.9 4.8 dynamic_update_slice.29
  165.7 4.8 dynamic_update_slice.29
  176.4 4.8 dynamic_update_slice.29
  187.2 4.8 dynamic_update_slice.29
  198.0 4.8 dynamic_update_slice.29
  208.7 4.8 dynamic_update_slice.29
  219.5 4.8 dynamic_update_slice.29
  225.7 2.1 all-gather.5
  228.6 11.5 %all-gather.6 = bf16[4,514,128]{2,1,0:T(8,128)(2,1)S(1)} all-gather(bf16[1,514,128]{2,1,0:T(8,128)(2,1)S(1)} %maximum_bitcast_fusion.1), channel_id=3, replica_groups=mesh['sp_0'=4,'sp_1'=4,'sp_2'=2,'tp'=4] {'sp_1'}, dimensions={0}, use_global_device_ids=true | all-gather | bytes 657920 | tf_op jit(solution)/shard_map/all_gather | solution.py:35
  241.5 10.9 %all-gather.7 = bf16[4,514,128]{2,1,0:T(8,128)(2,1)S(1)} all-gather(bf16[1,514,128]{2,1,0:T(8,128)(2,1)S(1)} %maximum_bitcast_fusion.2), channel_id=4, replica_groups=mesh['sp_0'=4,'sp_1'=4,'sp_2'=2,'tp'=4] {'sp_0'}, dimensions={0}, use_global_device_ids=true | all-gather | bytes 657920 | tf_op jit(solution)/shard_map/all_gather | solution.py:35
  253.3 1.9 add_exponential_fusion.1
  255.2 2.4 reshape.954
  258.5 1.2 copy.247
  259.8 2.4 reshape.977
  263.0 1.9 add_exponential_fusion
  264.9 1.2 copy.252
  266.2 1.5 fusion.141
  267.7 1.5 fusion.95
  270.5 1.4 fusion.135
  273.0 1.3 fusion.191
  274.4 3.3 add_convert_fusion
  279.7 94.6 %all-reduce.8.cloned.1.call-done = bf16[1024,2048]{1,0:T(8,128)(2,1)} async-done(((bf16[1024,2048]{1,0:T(8,128)(2,1)}), bf16[1024,2048]{1,0:T(8,128)(2,1)}) %all-reduce.8.cloned.1.call-update) | async-done | bytes 4194320 | tf_op jit(solution)/shard_map/psum | solution.py:280
  374.3 3.2 fusion.74
  377.8 6.0 %multiply_reduce_fusion = (f32[1024]{0:T(1024)S(1)}, f32[1024,2048]{1,0:T(8,128)}) fusion(f32[2048]{0:T(1024)S(1)} %convert_element_type.718, f32[1024]{0:T(1024)S(1)} %add_rsqrt_fusion.3, bf16[1024,2048]{1,0:T(8,128)(2,1)S(1)} %copy-done.2, bf16[1024,2048]{1,0:T(8,128)(2,1)} %param.29), kind=kLoop, calls=%fused_computation.98 | loop fusion | flops 14679040 | bytes 16793600 | tf_op jit(solution)/shard_map/reduce_sum | solution.py:186
  383.8 5.8 %copy.254 = bf16[16,2,64,1408]{3,2,1,0:T(8,128)(2,1)} copy(bf16[16,2,64,1408]{3,2,0,1:T(8,128)(2,1)} %bitcast.557) | data formatting | bytes 11534336 | tf_op jit(solution)/shard_map/transpose | solution.py:89
  389.6 12.6 %fusion.79 = f32[1024,1408]{1,0:T(8,128)} fusion(bf16[2048,2816]{1,0:T(8,128)(2,1)} %all-gather.12.cloned.1.call-done, f32[1024,2048]{1,0:T(8,128)} %get-tuple-element.310, f32[2048]{0:T(1024)S(1)} %convert_element_type.719, f32[1024]{0:T(1024)S(1)} %add_rsqrt_fusion.2), kind=kOutput, calls=%fused_computation.102 | convolution fusion | flops 5911871488 | bytes 19935232 | tf_op jit(solution)/shard_map/dot_general | solution.py:284
  402.2 21.5 %fusion.86 = bf16[1024,2048]{1,0:T(8,128)(2,1)} fusion(bf16[2048,1408]{1,0:T(8,128)(2,1)} %bitcast.558, f32[1024,1408]{1,0:T(8,128)} %fusion.79, bf16[2048,2816]{1,0:T(8,128)(2,1)} %all-gather.12.cloned.1.call-done, f32[1024,2048]{1,0:T(8,128)} %get-tuple-element.310, f32[2048]{0:T(1024)S(1)} %convert_element_type.719, f32[1024]{0:T(1024)S(1)} %add_rsqrt_fusion.2), kind=kOutput, calls=%fused_computation.106 | convolution fusion | flops 11828199424 | bytes 29896704 | tf_op jit(solution)/shard_map/dot_general | solution.py:290
  423.7 46.8 %reduce-scatter.2.cloned.1.call-done = bf16[256,2048]{1,0:T(8,128)(2,1)} async-done(((bf16[1024,2048]{1,0:T(8,128)(2,1)}), bf16[256,2048]{1,0:T(8,128)(2,1)}) %reduce-scatter.2.cloned.1.call-update) | async-done | bytes 1048592 | tf_op jit(solution)/shard_map/reduce_scatter | solution.py:289
  470.6 1.5 fusion.90
  472.1 3.3 fusion.93
  (421 shorter events, 112.6 us)
Async XLA Ops:
  7.4 265.7 %copy-start = (bf16[256,2048]{1,0:T(8,128)(2,1)S(1)}, bf16[256,2048]{1,0:T(8,128)(2,1)}, u32[]{:S(2)}) copy-start(bf16[256,2048]{1,0:T(8,128)(2,1)} %param.46) | copy-start | bytes 3145732
  7.4 31.6 %copy-start.12 = (bf16[256]{0:T(256)(128)(2,1)S(1)}, bf16[256]{0:T(256)(128)(2,1)}, u32[]{:S(2)}) copy-start(bf16[256]{0:T(256)(128)(2,1)} %param.45) | copy-start | bytes 1540
  7.4 270.4 %all-gather.14.cloned.1.call-start = ((), (), s32[]{:S(2)}) async-start(), calls=%async_computation.4 | async-start | bytes 3063808 | tf_op jit(solution)/shard_map/all_gather | solution.py:86
  8.1 366.2 %all-reduce.8.cloned.1.call-start = ((), (), s32[]{:S(2)}) async-start(), calls=%async_computation.1 | async-start | bytes 8388608 | tf_op jit(solution)/shard_map/psum | solution.py:280
  9.0 32.0 %collective-permute-start = (bf16[3,256]{0,1:T(8,128)(2,1)S(1)}, bf16[3,256]{0,1:T(8,128)(2,1)S(1)}, u32[]{:S(2)}, u32[]{:S(2)}) collective-permute-start(bf16[3,256]{0,1:T(8,128)(2,1)S(1)} %copy.225), channel_id=1, source_target_pairs={{0,4},{4,8},{8,12},{12,16},{16,20},{20,24},{24,28},{28,32},{32,36}... | collective-permute-start | bytes 4616 | tf_op jit(solution)/shard_map/ppermute | solution.py:18
  14.7 25.6 %collective-permute-start.1 = (bf16[3,2,128]{2,0,1:T(4,128)(2,1)S(1)}, bf16[3,2,128]{2,0,1:T(4,128)(2,1)S(1)}, u32[]{:S(2)}, u32[]{:S(2)}) collective-permute-start(bf16[3,2,128]{2,0,1:T(4,128)(2,1)S(1)} %slice.452), channel_id=1, source_target_pairs={{0,4},{4,8},{8,12},{12,16},{16,20},{20,24},{24,28},{28,32},{32,36}... | collective-permute-start | bytes 4616 | tf_op jit(solution)/shard_map/ppermute | solution.py:18
  17.7 0.8 copy-start.5
  18.5 27.4 %collective-permute-start.2 = (bf16[3,2,128]{2,0,1:T(4,128)(2,1)S(1)}, bf16[3,2,128]{2,0,1:T(4,128)(2,1)S(1)}, u32[]{:S(2)}, u32[]{:S(2)}) collective-permute-start(bf16[3,2,128]{2,0,1:T(4,128)(2,1)S(1)} %slice.458), channel_id=1, source_target_pairs={{0,4},{4,8},{8,12},{12,16},{16,20},{20,24},{24,28},{28,32},{32,36}... | collective-permute-start | bytes 4616 | tf_op jit(solution)/shard_map/ppermute | solution.py:18
  23.0 111.7 %collective-permute-start.3 = (bf16[3,256]{0,1:T(8,128)(2,1)S(1)}, bf16[3,256]{0,1:T(8,128)(2,1)S(1)}, u32[]{:S(2)}, u32[]{:S(2)}) collective-permute-start(bf16[3,256]{0,1:T(8,128)(2,1)S(1)} %copy.239), channel_id=1, source_target_pairs={{0,4},{4,8},{8,12},{12,16},{16,20},{20,24},{24,28},{28,32},{32,36}... | collective-permute-start | bytes 4616 | tf_op jit(solution)/shard_map/ppermute | solution.py:18
  252.5 0.8 copy-start.4
  266.2 5.7 %copy-start.3 = (f32[1024,1,2,128]{0,3,2,1:T(8,128)S(1)}, f32[1024,1,2,128]{0,3,2,1:T(8,128)}, u32[]{:S(2)}) copy-start(f32[1024,1,2,128]{0,3,2,1:T(8,128)} %reshape.977) | copy-start | bytes 3145732
  272.7 1.7 copy-start.6
  277.6 0.9 copy-start.7
  277.6 1.0 copy-start.8
  277.6 2.1 copy-start.9
  277.6 2.1 copy-start.10
  277.7 106.1 %all-gather.16.cloned.1.call-start = ((), (), s32[]{:S(2)}) async-start(), calls=%async_computation.5 | async-start | bytes 8650752 | tf_op jit(solution)/shard_map/all_gather | solution.py:86
  278.4 111.1 %all-gather.12.cloned.1.call-start = ((), (), s32[]{:S(2)}) async-start(), calls=%async_computation.2 | async-start | bytes 11894784 | tf_op jit(solution)/shard_map/all_gather | solution.py:70
  279.4 191.1 %reduce-scatter.2.cloned.1.call-start = ((), (), s32[]{:S(2)}) async-start(), calls=%async_computation.3 | async-start | bytes 5242880 | tf_op jit(solution)/shard_map/reduce_scatter | solution.py:289
  374.3 3.4 copy-start.2
  402.2 21.6 %copy-start.11 = (bf16[2048]{0:T(1024)(128)(2,1)S(1)}, bf16[2048]{0:T(1024)(128)(2,1)}, u32[]{:S(2)}) copy-start(bf16[2048]{0:T(1024)(128)(2,1)} %param.53) | copy-start | bytes 12292
  402.2 73.2 %copy-start.1 = (bf16[256,2048]{1,0:T(8,128)(2,1)S(1)}, bf16[256,2048]{1,0:T(8,128)(2,1)}, u32[]{:S(2)}) copy-start(bf16[256,2048]{1,0:T(8,128)(2,1)} %param.46) | copy-start | bytes 3145732
Sparse Core Ops, SparseCore 0:
  10.3 49.5 all-gather.13
  280.1 23.3 all-gather.15
  305.8 61.5 all-gather.11
Sparse Core Ops, SparseCore 1:
  277.7 96.5 all-reduce.7
  423.8 46.7 reduce-scatter.1
where the time goes:
time: 490 us; the launch traced here: 482 us
  waiting for transfers between devices  143 us (29%)
  local copies, waits for them, and re-layouts  137 us (28%)
  matrix products  104 us (21%)
  other arithmetic  45 us (9%)
  blocking collectives  24.6 us (5%)
  between operations  15.1 us (3%)
  starting transfers between devices  12.4 us (3%)
    psum x1, waiting for transfers between devices, local(): mix = lax.psum(partial_value.astype(jnp.bfloat16), 'tp').astype(jnp.float32)  94.6 us
    dynamic_update_slice x32, local copies, waits for them, and re-layouts, block_pass(): end_state, (outputs, cumulative) = lax.scan(one_block, start_state, blocked)  83.5 us
    reduce_scatter x1, waiting for transfers between devices, local(): lax.psum_scatter(lax.dot_general(hidden, down_full, (((1,), (1,)), ((), (...  46.8 us
    all_gather x3, blocking collectives, collected_together(): both, at, found = (lax.all_gather(jnp.concatenate(lines), axis), 0, {})  24.6 us
    dot_general x1, matrix products, local(): lax.dot_general(hidden, down_full, (((1,), (1,)), ((), ())), preferred_el...  21.5 us
    dot_general x16, matrix products, one_block(): jnp.einsum('ghls,sghp->lghp', weights, block_values, preferred_element_ty...  17.7 us
    dot_general x16, matrix products, one_block(): jnp.einsum('lghp,lgn->ghpn', scaled.astype(jnp.bfloat16), block_keys, pre...  16.3 us
    dynamic_slice x48, local copies, waits for them, and re-layouts, block_pass(): end_state, (outputs, cumulative) = lax.scan(one_block, start_state, blocked)  15.4 us
  transfers between devices with their start and end apart: 9, of which 2 were waited for; matrix products, arithmetic and copies ran while one was open for 51% of the time, Pallas kernels for 0%

commit v1 on v0

v1 whole, which is shorter than its diff:
```python
import functools

import jax
import jax.numpy as jnp
from jax import lax
from jax.experimental import pallas as pl
from jax.experimental.pallas import tpu as pltpu
from jax.sharding import Mesh
from jax.sharding import PartitionSpec as P

BLOCK = 128
ROWS = 1024
NBLK = ROWS // BLOCK
SP = ("sp_0", "sp_1", "sp_2")
SP_TP = ("sp_0", "sp_1", "sp_2", "tp")
EPS = 1e-06
MESH = pl.DeviceIdType.MESH
F32 = jnp.float32
BF16 = jnp.bfloat16


def dot(a, b, contract=((1,), (0,)), precision=None):
    return lax.dot_general(
        a, b, (contract, ((), ())), preferred_element_type=F32, precision=precision
    )


def silu(v):
    return v * jax.nn.sigmoid(v)


def spread(m):
    rows = m.shape[0]
    low = lax.broadcasted_iota(jnp.int32, (rows, 128), 1) < 64
    cols = [jnp.broadcast_to(m[:, h : h + 1], (rows, 128)) for h in range(6)]
    return (
        jnp.where(low, cols[0], cols[1]),
        jnp.where(low, cols[2], cols[3]),
        cols[4],
        cols[5],
    )


def block_rows(b):
    return pl.ds(pl.multiple_of(b * BLOCK, BLOCK), BLOCK)


def ssm_kernel(
    sh, lh, ks, qs, sg, lg, sst, lst, stap, ltap, ktap, qtap, sdec, ldec, sgain, lgain,
    out,
    xs, xl, kc, qc, dtt, ct, ccol, dcol, hloc, eoff, inside,
    halo, mine, mine_tot, sbuf, sib, sib_tot, ysend, ytot_send, yrec, ytot, zsend, ztot_send, zrec, ztot, esend, ebuf,
    hs_sem, hr_sem, s1_sem, r1_sem, ys_sem, yr_sem, zs_sem, zr_sem, s4_sem, r4_sem,
):
    z = lax.axis_index("sp_0")
    y = lax.axis_index("sp_1")
    c = lax.axis_index("sp_2")
    sp = (z * 4 + y) * 2 + c
    nxt = lax.rem(sp + 1, 32)
    prv = lax.rem(sp + 31, 32)

    def at_sp(i):
        return {"sp_0": i // 8, "sp_1": lax.rem(i // 2, 4), "sp_2": lax.rem(i, 2)}

    ypeers = [{"sp_1": lax.rem(y + d, 4)} for d in (1, 2, 3)]
    zpeers = [{"sp_0": lax.rem(z + d, 4)} for d in (1, 2, 3)]
    sibling = {"sp_2": 1 - c}
    barrier = pltpu.get_barrier_semaphore()
    peers = [at_sp(nxt), at_sp(prv), sibling] + ypeers + zpeers
    for peer in peers:
        pl.semaphore_signal(barrier, inc=1, device_id=peer, device_id_type=MESH)
    pl.semaphore_wait(barrier, len(peers))

    sources = (sh, lh, ks, qs)
    halo_copies = [
        pltpu.make_async_remote_copy(
            src_ref=src.at[pl.ds(ROWS - 16, 16)], dst_ref=halo.at[i],
            send_sem=hs_sem.at[i], recv_sem=hr_sem.at[i],
            device_id=at_sp(nxt), device_id_type=MESH,
        )
        for i, src in enumerate(sources)
    ]
    for copy in halo_copies:
        copy.start()

    dtt[...] = jnp.zeros_like(dtt)
    dtt[0:4, :] = jax.nn.softplus(sst[...])
    dtt[4:6, :] = jax.nn.softplus(lst[...])
    ct[...] = jnp.zeros_like(ct)
    for h in range(6):
        d = sdec[h] if h < 4 else ldec[h - 4]
        rate = jnp.exp(jnp.full((1, ROWS), d, F32))
        ct[h : h + 1, :] = -dtt[h : h + 1, :] * rate
    tr = lax.broadcasted_iota(jnp.int32, (BLOCK, BLOCK), 0)
    tc = lax.broadcasted_iota(jnp.int32, (BLOCK, BLOCK), 1)
    upper = (tr <= tc).astype(F32)
    low = tc < 64
    causal = tc <= tr

    def sums(b, _):
        rows = block_rows(b)
        cum = dot(ct[:, rows], upper, precision=lax.Precision.HIGHEST)
        ct[:, rows] = cum
        pad = jnp.zeros((BLOCK - 8, BLOCK), F32)
        ccol[rows, :] = jnp.concatenate([cum, pad], axis=0).T
        dcol[rows, :] = jnp.concatenate([dtt[:, rows], pad], axis=0).T
        return 0

    lax.fori_loop(0, NBLK, sums, 0)

    taps = (stap, ltap, ktap, qtap)
    dests = (xs, xl, kc, qc)

    def conv_of(ext, tap):
        acc = jnp.zeros((BLOCK, 256), F32)
        for k in range(4):
            shifted = ext if k == 3 else pltpu.roll(ext, 3 - k, 0)
            acc = acc + tap[k : k + 1, :].astype(F32) * shifted[16:, :]
        return silu(acc).astype(BF16)

    def conv_block(b, _):
        start = pl.multiple_of(b * BLOCK - 16, 16)
        for src, tap, dst in zip(sources, taps, dests):
            ext = src[pl.ds(start, BLOCK + 16), :].astype(F32)
            dst[block_rows(b), :] = conv_of(ext, tap)
        return 0

    lax.fori_loop(1, NBLK, conv_block, 0)
    for copy in halo_copies:
        copy.wait()
    keep = jnp.where(sp == 0, 0.0, 1.0)
    for i, (src, tap, dst) in enumerate(zip(sources, taps, dests)):
        before = halo[i].astype(F32) * keep
        ext = jnp.concatenate([before, src[0:BLOCK, :].astype(F32)], axis=0)
        dst[0:BLOCK, :] = conv_of(ext, tap)

    mine[...] = jnp.zeros_like(mine)
    mine_tot[...] = jnp.zeros_like(mine_tot)

    def states(b, _):
        rows = block_rows(b)
        cb = ccol[rows, :]
        last = cb[BLOCK - 1 : BLOCK, :]
        scale = spread(dcol[rows, :] * jnp.exp(last - cb))
        xsb = xs[rows, :].astype(F32)
        xlb = xl[rows, :].astype(F32)
        us = jnp.concatenate([xsb[:, :128] * scale[0], xsb[:, 128:] * scale[1]], axis=1)
        ul = jnp.concatenate([xlb[:, :128] * scale[2], xlb[:, 128:] * scale[3]], axis=1)
        fresh_s = dot(kc[rows, 0:128], us.astype(BF16), ((0,), (0,)))
        fresh_l = dot(kc[rows, 128:256], ul.astype(BF16), ((0,), (0,)))
        state = mine[...]
        tot = mine_tot[...]
        hloc[b] = state
        eoff[b] = jnp.exp(tot)
        step = jnp.concatenate(spread(jnp.broadcast_to(last, (8, 128))), axis=1)
        mine[...] = state * jnp.exp(step)[0:1, :] + jnp.concatenate([fresh_s, fresh_l], axis=1)
        mine_tot[...] = tot + step
        return 0

    lax.fori_loop(0, NBLK, states, 0)

    sbuf[...] = mine[...].astype(BF16)
    r1 = [
        pltpu.make_async_remote_copy(
            src_ref=src, dst_ref=dst, send_sem=s1_sem.at[i], recv_sem=r1_sem.at[i],
            device_id=sibling, device_id_type=MESH,
        )
        for i, (src, dst) in enumerate(((sbuf, sib), (mine_tot, sib_tot)))
    ]
    for copy in r1:
        copy.start()

    def intra(b, _):
        rows = block_rows(b)
        cb = ccol[rows, :]
        parts = []
        for g, x in ((0, xs), (1, xl)):
            lanes = slice(g * 128, g * 128 + 128)
            scores = dot(qc[rows, lanes], kc[rows, lanes], ((1,), (1,)))
            heads = []
            for h in range(4) if g == 0 else range(4, 6):
                gap = jnp.broadcast_to(cb[:, h : h + 1], (BLOCK, BLOCK)) - ct[h : h + 1, rows]
                decay = jnp.exp(jnp.where(causal, gap, -1e30))
                w = (scores * decay * dtt[h : h + 1, rows]).astype(BF16)
                at = (h // 2 if g == 0 else h - 4) * 128
                heads.append(dot(w, x[rows, at : at + 128]))
            if g == 0:
                parts += [jnp.where(low, heads[0], heads[1]), jnp.where(low, heads[2], heads[3])]
            else:
                parts += heads
        inside[rows, :] = jnp.concatenate(parts, axis=1)
        return 0

    lax.fori_loop(0, 2, intra, 0)
    for copy in r1:
        copy.wait()

    half = pl.ds(pl.multiple_of(c * 64, 64), 64)
    my_half = mine[half, :]
    sib_half = sib[half, :].astype(F32)
    first = c == 0
    t_me = mine_tot[...]
    t_sib = sib_tot[...]
    early = jnp.where(first, my_half, sib_half)
    late = jnp.where(first, sib_half, my_half)
    t_late = jnp.where(first, t_sib, t_me)
    chip = early * jnp.exp(t_late)[0:1, :] + late
    chip_tot = t_me + t_sib
    ysend[...] = chip.astype(BF16)
    ytot_send[...] = chip_tot
    def peer_copies(send, tot_send, rec, tot_rec, sems, peers_):
        ss, rs = sems
        made = []
        for i, peer in enumerate(peers_):
            for j, (src, dst) in enumerate(((send, rec.at[i]), (tot_send, tot_rec.at[i]))):
                made.append(pltpu.make_async_remote_copy(
                    src_ref=src, dst_ref=dst, send_sem=ss.at[2 * i + j], recv_sem=rs.at[2 * i + j],
                    device_id=peer, device_id_type=MESH,
                ))
        return made

    r2 = peer_copies(ysend, ytot_send, yrec, ytot, (ys_sem, yr_sem), ypeers)
    for copy in r2:
        copy.start()
    lax.fori_loop(2, 5, intra, 0)
    for copy in r2:
        copy.wait()

    def before_of(pos, rec, tot_rec):
        e = jnp.zeros((64, 512), F32)
        t = jnp.zeros((8, 512), F32)
        for d in (3, 2, 1):
            valid = d <= pos
            e = jnp.where(valid, e * jnp.exp(tot_rec[d - 1])[0:1, :] + rec[d - 1].astype(F32), e)
            t = jnp.where(valid, t + tot_rec[d - 1], t)
        return e, t

    ey, ty = before_of(y, yrec, ytot)
    plane = ey * jnp.exp(chip_tot)[0:1, :] + chip
    plane_tot = ty + chip_tot
    for e in (1, 2, 3):
        valid = y + e <= 3
        plane = jnp.where(valid, plane * jnp.exp(ytot[3 - e])[0:1, :] + yrec[3 - e].astype(F32), plane)
        plane_tot = jnp.where(valid, plane_tot + ytot[3 - e], plane_tot)
    zsend[...] = plane.astype(BF16)
    ztot_send[...] = plane_tot
    r3 = peer_copies(zsend, ztot_send, zrec, ztot, (zs_sem, zr_sem), zpeers)
    for copy in r3:
        copy.start()
    lax.fori_loop(5, NBLK, intra, 0)
    for copy in r3:
        copy.wait()
    ez, _ = before_of(z, zrec, ztot)
    entering = ez * jnp.exp(ty)[0:1, :] + ey
    esend[...] = entering
    r4 = pltpu.make_async_remote_copy(
        src_ref=esend, dst_ref=ebuf.at[half], send_sem=s4_sem, recv_sem=r4_sem,
        device_id=sibling, device_id_type=MESH,
    )
    r4.start()
    r4.wait()
    own = esend[...]
    enter_rows = []
    for i in range(2):
        arrived = ebuf[i * 64 : i * 64 + 64, :]
        enter_rows.append(jnp.where(c == i, own, arrived))
    enter = jnp.concatenate(enter_rows, axis=0)
    second = enter * jnp.exp(t_sib)[0:1, :] + sib[...].astype(F32)
    mine[...] = jnp.where(first, enter, second)

    def finish(b, _):
        rows = block_rows(b)
        state = (hloc[b] + eoff[b][0:1, :] * mine[...]).astype(BF16)
        grow = spread(jnp.exp(ccol[rows, :]))
        carried = [dot(qc[rows, g * 128 : g * 128 + 128], state[:, g * 256 : g * 256 + 256]) for g in (0, 1)]
        for i in range(4):
            g, at = i // 2, (i % 2) * 128
            gate_ref = sg if g == 0 else lg
            gain_ref = sgain if g == 0 else lgain
            v = inside[rows, i * 128 : i * 128 + 128] + carried[g][:, at : at + 128] * grow[i]
            v = v * silu(gate_ref[rows, at : at + 128].astype(F32))
            sq = v * v
            if g == 0:
                s0 = jnp.sum(jnp.where(low, sq, 0.0), axis=1, keepdims=True)
                s1 = jnp.sum(jnp.where(low, 0.0, sq), axis=1, keepdims=True)
                inv = jnp.where(low, lax.rsqrt(s0 / 64 + EPS), lax.rsqrt(s1 / 64 + EPS))
            else:
                inv = lax.rsqrt(jnp.sum(sq, axis=1, keepdims=True) / 128 + EPS)
            v = v * inv * gain_ref[:, at : at + 128].astype(F32)
            out[rows, i * 128 : i * 128 + 128] = v.astype(BF16)
        return 0

    lax.fori_loop(0, NBLK, finish, 0)


def ssm(*operands):
    vm = pl.BlockSpec(memory_space=pltpu.VMEM)
    sm = pl.BlockSpec(memory_space=pltpu.SMEM)
    dma = pltpu.SemaphoreType.DMA
    rows_bf = pltpu.VMEM((ROWS, 256), BF16)
    return pl.pallas_call(
        ssm_kernel,
        name="ssm",
        out_shape=jax.ShapeDtypeStruct((ROWS, 512), BF16),
        in_specs=[vm] * 12 + [sm] * 2 + [vm] * 2,
        out_specs=vm,
        scratch_shapes=[
            rows_bf, rows_bf, rows_bf, rows_bf,
            pltpu.VMEM((8, ROWS), F32), pltpu.VMEM((8, ROWS), F32),
            pltpu.VMEM((ROWS, 128), F32), pltpu.VMEM((ROWS, 128), F32),
            pltpu.VMEM((NBLK, 128, 512), F32), pltpu.VMEM((NBLK, 8, 512), F32),
            pltpu.VMEM((ROWS, 512), F32),
            pltpu.VMEM((4, 16, 256), BF16),
            pltpu.VMEM((128, 512), F32), pltpu.VMEM((8, 512), F32),
            pltpu.VMEM((128, 512), BF16), pltpu.VMEM((128, 512), BF16), pltpu.VMEM((8, 512), F32),
            pltpu.VMEM((64, 512), BF16), pltpu.VMEM((8, 512), F32),
            pltpu.VMEM((3, 64, 512), BF16), pltpu.VMEM((3, 8, 512), F32),
            pltpu.VMEM((64, 512), BF16), pltpu.VMEM((8, 512), F32),
            pltpu.VMEM((3, 64, 512), BF16), pltpu.VMEM((3, 8, 512), F32),
            pltpu.VMEM((64, 512), F32), pltpu.VMEM((128, 512), F32),
            dma((4,)), dma((4,)), dma((2,)), dma((2,)), dma((6,)), dma((6,)), dma((6,)), dma((6,)), dma, dma,
        ],
        compiler_params=pltpu.CompilerParams(collective_id=0, has_side_effects=True, vmem_limit_bytes=48 * 1024 * 1024),
        cost_estimate=pl.CostEstimate(flops=4_000_000_000, bytes_accessed=5_000_000, transcendentals=0),
    )(*operands)


def unit_rms(values):
    return values * lax.rsqrt(jnp.mean(values * values, axis=-1, keepdims=True) + EPS)


def local(
    residual, small_heads, large_heads, state_keys, state_queries, small_gate, large_gate,
    small_step, large_step, small_taps, large_taps, key_taps, query_taps, small_decay, large_decay,
    small_gain, large_gain, small_out, large_out, mixer_gain, ffn_in_gain,
    gate_proj, up_proj, down_proj, ffn_out_gain,
):
    length = residual.shape[0]
    weights = lax.all_gather(
        jnp.concatenate([gate_proj, up_proj, down_proj], axis=1), SP, axis=0, tiled=True
    )
    ff = gate_proj.shape[1]
    normed = ssm(
        small_heads, large_heads, state_keys.reshape(length, 256), state_queries.reshape(length, 256),
        small_gate, large_gate, small_step.T, large_step.T, small_taps, large_taps,
        key_taps.reshape(4, 256), query_taps.reshape(4, 256), small_decay, large_decay,
        small_gain.reshape(1, 256), large_gain.reshape(1, 256),
    )
    partial_value = jnp.dot(normed[:, :256], small_out, preferred_element_type=F32)
    partial_value = partial_value + jnp.dot(normed[:, 256:], large_out, preferred_element_type=F32)
    mix = lax.psum_scatter(partial_value.astype(BF16), "tp", scatter_dimension=0, tiled=True).astype(F32)
    share = length // lax.axis_size("tp")
    own = lax.dynamic_slice_in_dim(residual, lax.axis_index("tp") * share, share, 0).astype(F32)
    mixed = own + unit_rms(mix) * mixer_gain.astype(F32)
    normed_in = (unit_rms(mixed) * ffn_in_gain.astype(F32)).astype(BF16)
    normed_in = lax.all_gather(normed_in, "tp", axis=0, tiled=True)
    gate = jnp.dot(normed_in, weights[:, :ff], preferred_element_type=F32)
    up_values = jnp.dot(normed_in, weights[:, ff : 2 * ff], preferred_element_type=F32)
    hidden = (jax.nn.silu(gate) * up_values).astype(BF16)
    ffn = lax.psum_scatter(
        lax.dot_general(
            hidden, weights[:, 2 * ff :], (((1,), (1,)), ((), ())), preferred_element_type=F32
        ).astype(BF16),
        "tp", scatter_dimension=0, tiled=True,
    ).astype(F32)
    updated = mixed + 0.5 * unit_rms(ffn) * ffn_out_gain.astype(F32)
    return updated.astype(BF16)


def solution(mesh):
    torus = Mesh(mesh.devices.reshape(4, 4, 2, mesh.shape["tp"]), ("sp_0", "sp_1", "sp_2", "tp"))
    in_specs = (
        P(SP, None), P(SP, "tp"), P(SP, "tp"), P(SP, "tp", None), P(SP, "tp", None),
        P(SP, "tp"), P(SP, "tp"), P(SP, "tp"), P(SP, "tp"),
        P(None, "tp"), P(None, "tp"), P(None, "tp", None), P(None, "tp", None),
        P("tp"), P("tp"), P("tp"), P("tp"), P("tp", None), P("tp", None),
        P(), P(), P(SP, "tp"), P(SP, "tp"), P(SP, "tp"), P(),
    )
    return jax.shard_map(local, mesh=torus, in_specs=in_specs, out_specs=P(SP_TP, None), check_vma=False)
```

time: 490 us -> 326 us (0.67); the launches traced: 482 us -> 325 us
  local copies, waits for them, and re-layouts: 137 us -> 13 us
  waiting for transfers between devices: 143 us -> 214 us
  matrix products: 104 us -> 38.8 us
  Pallas kernels: 0 us -> 33.3 us
  other arithmetic: 45 us -> 12.4 us
  blocking collectives: 24.6 us -> 0 us
  starting transfers between devices: 12.4 us -> 0.31 us
    all_gather x3 -> x2, waiting for transfers between devices: 0.02 us -> 124 us  [the longest x1 77.2 us: local(): lax.all_gather(jnp.concatenate([gate_proj, up_proj, down_proj], axis=1),...]
    psum x1 -> x0, waiting for transfers between devices: 94.6 us -> none  [local(): mix = lax.psum(partial_value.astype(jnp.bfloat16), 'tp').astype(jnp.float32)]
    dynamic_update_slice x32 -> x0, local copies, waits for them, and re-layouts: 83.5 us -> none  [block_pass(): end_state, (outputs, cumulative) = lax.scan(one_block, start_state, blocked)]
    dot_general x70 -> x4, matrix products: 104 us -> 38.8 us  [the longest x1 22.7 us: local(): lax.dot_general(hidden, weights[:, 2 * ff:], (((1,), (1,)), ((), ())), pr...]
    reduce_scatter x1 -> x2, waiting for transfers between devices: 46.8 us -> 90.3 us  [the longest x1 45.2 us: local(): lax.psum_scatter(lax.dot_general(hidden, weights[:, 2 * ff:], (((1,), (1,...]
    pallas_call x0 -> x1, Pallas kernels: none -> 33.3 us  [ssm(): pl.pallas_call(ssm_kernel, name='ssm', out_shape=jax.ShapeDtypeStruct((RO...]
    all_gather x3 -> x0, blocking collectives: 24.6 us -> none  [collected_together(): both, at, found = (lax.all_gather(jnp.concatenate(lines), axis), 0, {})]
    dynamic_slice x48 -> x0, local copies, waits for them, and re-layouts: 15.4 us -> none  [block_pass(): end_state, (outputs, cumulative) = lax.scan(one_block, start_state, blocked)]
  transfers between devices with their start and end apart: 9 -> 4, of which waited for: 2 -> 4; matrix products, arithmetic and copies ran while one was open for 51% -> 0% of each run, Pallas kernels for 0% -> 0%
where the time goes in v1:
time: 326 us; the launch traced here: 325 us
  waiting for transfers between devices  214 us (66%)
  matrix products  38.8 us (12%)
  Pallas kernels  33.3 us (10%)
  between operations  13.3 us (4%)
  local copies, waits for them, and re-layouts  13 us (4%)
  other arithmetic  12.4 us (4%)
    all_gather x1, waiting for transfers between devices, local(): lax.all_gather(jnp.concatenate([gate_proj, up_proj, down_proj], axis=1),...  77.2 us
    all_gather x1, waiting for transfers between devices, local(): normed_in = lax.all_gather(normed_in, 'tp', axis=0, tiled=True)  46.8 us
    reduce_scatter x1, waiting for transfers between devices, local(): lax.psum_scatter(lax.dot_general(hidden, weights[:, 2 * ff:], (((1,), (1,...  45.2 us
    reduce_scatter x1, waiting for transfers between devices, local(): lax.psum_scatter(partial_value.astype(BF16), 'tp', scatter_dimension=0, t...  45.1 us
    pallas_call x1, Pallas kernels, ssm(): pl.pallas_call(ssm_kernel, name='ssm', out_shape=jax.ShapeDtypeStruct((RO...  33.3 us
    dot_general x1, matrix products, local(): lax.dot_general(hidden, weights[:, 2 * ff:], (((1,), (1,)), ((), ())), pr...  22.7 us
    dot_general x1, matrix products, local(): gate = jnp.dot(normed_in, weights[:, :ff], preferred_element_type=F32)  11.7 us
    unnamed x38, local copies, waits for them, and re-layouts  9.53 us
  transfers between devices with their start and end apart: 4, of which 4 were waited for; matrix products, arithmetic and copies ran while one was open for 0% of the time, Pallas kernels for 0%

profile of v1, /device:TPU:1, one launch (start us, length us, event | category | flops | bytes accessed | tf_op | source)
XLA Modules:
  0.0 325.4 jit_solution(1449966311935030156)
XLA Ops:
  6.5 0.0 copy-start
  6.5 0.0 reduce-scatter.3.cloned.1.call-start
  6.5 0.7 reshape.49.sgain
  7.3 0.7 reshape.50.lgain
  7.9 1.4 copy_bitcast_fusion
  9.3 0.7 copy_bitcast_fusion.2
  10.0 0.0 copy-start.1
  10.0 1.0 copy-done.1
  11.1 0.0 copy-start.2
  11.1 1.0 copy-done.2
  12.1 0.0 copy-start.3
  12.1 1.0 copy-done.3
  13.1 0.0 copy-start.4
  13.1 1.0 copy-done.4
  14.2 0.0 copy-start.5
  14.2 0.7 copy-done.5
  14.9 0.0 copy-start.6
  14.9 0.7 copy-done.6
  15.6 0.0 copy-start.7
  15.6 0.7 copy-done.7
  16.3 0.0 copy-start.8
  16.3 0.7 copy-done.8
  17.0 0.0 copy-start.9
  17.0 0.7 copy-done.9
  17.6 0.0 copy-start.10
  17.6 0.7 copy-done.10
  18.3 33.3 %ssm.1 = bf16[1024,512]{1,0:T(8,128)(2,1)S(1)} custom-call(bf16[1024,256]{1,0:T(8,128)(2,1)S(1)} %copy-done.1, bf16[1024,256]{1,0:T(8,128)(2,1)S(1)} %copy-done.2, bf16[1024,256]{1,0:T(8,128)(2,1)S(1)} %get-tuple-element.6.ks, bf16[1024,256]{1,0:T(8,128)(2,1)S(1)} %get-tuple-element.5.qs, bf16[1024,256]{1,0:T(8,128)(2,1)S(1)} %copy-done.3, ...), custom_call_target="tpu_custom_call" | custom-call | flops 4000000000 | bytes 5000000 | tf_op jit(solution)/shard_map/ssm/pallas_call | solution.py:301
  51.6 0.0 copy-done
  51.6 0.0 copy-start.12
  51.6 1.3 fusion.22
  52.9 0.0 copy-done.12
  52.9 3.2 add_convert_fusion
  56.1 0.0 copy-start.16
  56.1 0.0 copy-start.17
  56.1 0.0 reduce-scatter.3.cloned.1.call-update
  56.1 0.0 copy-start.13
  56.1 0.0 copy-start.14
  56.1 0.0 copy-start.15
  56.2 0.0 all-gather.3.cloned.1.call-start
  56.2 0.6 copy-done.16
  56.8 0.0 copy-done.17
  56.8 45.1 %reduce-scatter.3.cloned.1.call-done = bf16[256,2048]{1,0:T(8,128)(2,1)} async-done(((bf16[1024,2048]{1,0:T(8,128)(2,1)}), bf16[256,2048]{1,0:T(8,128)(2,1)}) %reduce-scatter.3.cloned.1.call-update) | async-done | bytes 1048592 | tf_op jit(solution)/shard_map/reduce_scatter | solution.py:351
  101.9 1.5 fusion.14
  103.4 2.2 multiply_reduce_fusion
  105.5 3.1 multiply_convert_fusion.1
  108.7 0.0 all-gather.3.cloned.1.call-update
  108.7 0.0 all-gather.5.cloned.1.call-start
  108.7 0.0 copy-done.13
  108.7 0.0 copy-done.14
  108.8 0.0 copy-done.15
  108.8 0.8 pad_maximum_fusion
  109.6 0.0 all-gather.5.cloned.1.call-update
  109.6 0.2 reduce-scatter.5.cloned.1.call-start
  109.9 46.8 %all-gather.3.cloned.1.call-done = bf16[1024,2048]{1,0:T(8,128)(2,1)} async-done(((bf16[256,2048]{1,0:T(8,128)(2,1)}), bf16[1024,2048]{1,0:T(8,128)(2,1)}) %all-gather.3.cloned.1.call-update) | async-done | bytes 4194320 | tf_op jit(solution)/shard_map/all_gather | solution.py:356
  156.7 77.2 %all-gather.5.cloned.1.call-done = bf16[2048,4224]{1,0:T(8,128)(2,1)} async-done(((bf16[64,4224]{1,0:T(8,128)(2,1)}), bf16[2048,4224]{1,0:T(8,128)(2,1)}) %all-gather.5.cloned.1.call-update) | async-done | bytes 17301520 | tf_op jit(solution)/shard_map/all_gather | solution.py:339
  233.8 11.7 %fusion.4 = f32[1024,1408]{1,0:T(8,128)} fusion(bf16[1024,2048]{1,0:T(8,128)(2,1)} %all-gather.3.cloned.1.call-done, bf16[2048,4224]{1,0:T(8,128)(2,1)} %all-gather.5.cloned.1.call-done), kind=kOutput, calls=%fused_computation.5 | convolution fusion | flops 5905580032 | bytes 15728640 | tf_op jit(solution)/shard_map/dot_general | solution.py:357
  245.5 22.7 %fusion.8 = bf16[1024,2048]{1,0:T(8,128)(2,1)} fusion(bf16[2048,4224]{1,0:T(8,128)(2,1)} %all-gather.5.cloned.1.call-done, f32[1024,1408]{1,0:T(8,128)} %fusion.4, bf16[1024,2048]{1,0:T(8,128)(2,1)} %all-gather.3.cloned.1.call-done), kind=kOutput, calls=%fused_computation.8 | convolution fusion | flops 11821907968 | bytes 25690112 | tf_op jit(solution)/shard_map/dot_general | solution.py:361
  268.2 0.0 copy-start.18
  268.2 0.0 reduce-scatter.5.cloned.1.call-update
  268.2 0.7 copy-done.18
  268.9 45.2 %reduce-scatter.5.cloned.1.call-done = bf16[256,2048]{1,0:T(8,128)(2,1)} async-done(((bf16[1024,2048]{1,0:T(8,128)(2,1)}), bf16[256,2048]{1,0:T(8,128)(2,1)}) %reduce-scatter.5.cloned.1.call-update) | async-done | bytes 1048592 | tf_op jit(solution)/shard_map/reduce_scatter | solution.py:360
  314.1 1.5 fusion.17
  315.6 0.0 copy-done.11
  315.6 3.3 %fusion.20 = bf16[256,2048]{1,0:T(8,128)(2,1)} fusion(bf16[256,2048]{1,0:T(8,128)(2,1)} %reduce-scatter.5.cloned.1.call-done, bf16[256,2048]{1,0:T(8,128)(2,1)S(1)} %copy-done.11, f32[2048]{0:T(1024)S(1)} %convert_multiply_fusion.4, f32[256]{0:T(256)S(1)} %add_rsqrt_fusion, f32[2048]{0:T(1024)S(1)} %convert_element_type.36, f32[256]{0:T(256)S(1)} %add_rsqrt_fusion.2, ...), kind=kLoop, calls=%fused_computation.20 | loop fusion | flops 5242880 | bytes 4212740 | tf_op jit(solution)/shard_map/convert_element_type | solution.py:367
  (7 shorter events, 0.0 us)
Async XLA Ops:
  6.5 45.0 %copy-start = (bf16[256,2048]{1,0:T(8,128)(2,1)S(1)}, bf16[256,2048]{1,0:T(8,128)(2,1)}, u32[]{:S(2)}) copy-start(bf16[256,2048]{1,0:T(8,128)(2,1)} %param.42) | copy-start | bytes 3145732
  6.5 95.3 %reduce-scatter.3.cloned.1.call-start = ((), (), s32[]{:S(2)}) async-start(), calls=%async_computation.2 | async-start | bytes 5242880 | tf_op jit(solution)/shard_map/reduce_scatter | solution.py:351
  10.0 1.0 copy-start.1
  11.1 1.0 copy-start.2
  12.1 1.0 copy-start.3
  13.1 1.0 copy-start.4
  14.2 0.7 copy-start.5
  14.9 0.7 copy-start.6
  15.6 0.7 copy-start.7
  16.3 0.7 copy-start.8
  17.0 0.7 copy-start.9
  17.6 0.7 copy-start.10
  51.6 1.3 copy-start.12
  56.1 0.7 copy-start.16
  56.1 0.7 copy-start.17
  56.1 52.6 %copy-start.13 = (bf16[64,1408]{1,0:T(8,128)(2,1)S(1)}, bf16[64,1408]{1,0:T(8,128)(2,1)}, u32[]{:S(2)}) copy-start(bf16[64,1408]{1,0:T(8,128)(2,1)} %param.48) | copy-start | bytes 540676
  56.1 52.6 %copy-start.14 = (bf16[64,1408]{1,0:T(8,128)(2,1)S(1)}, bf16[64,1408]{1,0:T(8,128)(2,1)}, u32[]{:S(2)}) copy-start(bf16[64,1408]{1,0:T(8,128)(2,1)} %param.47) | copy-start | bytes 540676
  56.1 52.6 %copy-start.15 = (bf16[64,1408]{1,0:T(8,128)(2,1)S(1)}, bf16[64,1408]{1,0:T(8,128)(2,1)}, u32[]{:S(2)}) copy-start(bf16[64,1408]{1,0:T(8,128)(2,1)} %param.46) | copy-start | bytes 540676
  56.2 100.5 %all-gather.3.cloned.1.call-start = ((), (), s32[]{:S(2)}) async-start(), calls=%async_computation.3 | async-start | bytes 5242880 | tf_op jit(solution)/shard_map/all_gather | solution.py:356
  108.7 125.2 %all-gather.5.cloned.1.call-start = ((), (), s32[]{:S(2)}) async-start(), calls=%async_computation.4 | async-start | bytes 17842176 | tf_op jit(solution)/shard_map/all_gather | solution.py:339
  109.6 204.5 %reduce-scatter.5.cloned.1.call-start = ((), (), s32[]{:S(2)}) async-start(), calls=%async_computation.5 | async-start | bytes 5242880 | tf_op jit(solution)/shard_map/reduce_scatter | solution.py:360
  268.2 0.7 copy-start.18
  268.2 47.4 %copy-start.11 = (bf16[256,2048]{1,0:T(8,128)(2,1)S(1)}, bf16[256,2048]{1,0:T(8,128)(2,1)}, u32[]{:S(2)}) copy-start(bf16[256,2048]{1,0:T(8,128)(2,1)} %reduce-scatter.3.cloned.1.call-done) | copy-start | bytes 3145732
Sparse Core Ops, SparseCore 0:
  56.2 45.5 reduce-scatter.2
  108.8 47.8 all-gather.2
  158.9 74.8 all-gather.4
  268.4 45.7 reduce-scatter.4

commit v2 on v1

--- a/solution.py
+++ b/solution.py
@@ -45,47 +45,148 @@
     return pl.ds(pl.multiple_of(b * BLOCK, BLOCK), BLOCK)
 
 
-def ssm_kernel(
-    sh, lh, ks, qs, sg, lg, sst, lst, stap, ltap, ktap, qtap, sdec, ldec, sgain, lgain,
+OWN = 256
+FF_DEV = 1408
+UP_COLS = pl.ds(0, 2 * FF_DEV)
+DOWN_COLS = pl.ds(2 * FF_DEV, FF_DEV)
+
+
+class Net:
+    def __init__(self, send_sems, recv_sems):
+        self.send_sems, self.recv_sems, self.used = send_sems, recv_sems, 0
+
+    def copy(self, src, dst, peer):
+        i = self.used
+        self.used += 1
+        return pltpu.make_async_remote_copy(
+            src_ref=src, dst_ref=dst, send_sem=self.send_sems.at[i], recv_sem=self.recv_sems.at[i],
+            device_id=peer, device_id_type=MESH,
+        )
+
+
+class Ring:
+    def __init__(self, net, axis, at, view, pieces=(None,)):
+        self.net, self.at, self.view = net, at, view
+        self.before, self.after = lax.rem(at + 3, 4), lax.rem(at + 1, 4)
+        self.up, self.down = {axis: self.after}, {axis: self.before}
+        self.ups = [net.copy(view(at, p), view(at, p), self.up) for p in pieces]
+        self.downs = [net.copy(view(at, p), view(at, p), self.down) for p in pieces[::-1]]
+        self.forwards = []
+
+    def start(self):
+        for pair in zip(self.ups, self.downs):
+            for copy in pair:
+                copy.start()
+
+    def forward(self):
+        self.ups[0].wait_recv()
+        here = self.view(self.before, 0)
+        self.forwards.append(self.net.copy(here, here, self.up))
+        self.forwards[-1].start()
+        self.downs[0].wait_recv()
+        here = self.view(self.after, 1)
+        self.forwards.append(self.net.copy(here, here, self.down))
+        self.forwards[-1].start()
+
+    def neighbours(self):
+        for copy in self.ups[1:] + self.downs[1:]:
+            copy.wait_recv()
+
+    def finish(self):
+        for copy in self.forwards:
+            copy.wait_recv()
+        for copy in self.ups + self.downs + self.forwards:
+            copy.wait_send()
+
+
+def layer_kernel(
+    residual, sh_in, lh_in, ks_in, qs_in, sg_in, lg_in, gate_in, up_in, down_in, so_in, lo_in,
+    steps, params, sdec, ldec,
     out,
+    sh, lh, ks, qs, sg, lg,
     xs, xl, kc, qc, dtt, ct, ccol, dcol, hloc, eoff, inside,
     halo, mine, mine_tot, sbuf, sib, sib_tot, ysend, ytot_send, yrec, ytot, zsend, ztot_send, zrec, ztot, esend, ebuf,
-    hs_sem, hr_sem, s1_sem, r1_sem, ys_sem, yr_sem, zs_sem, zr_sem, s4_sem, r4_sem,
+    heads, chans, weights, projs, res, mixed, rows_in, hidden, parts_out, relay, relay_sum, from_left, from_right,
+    send_sems, recv_sems, load_sems,
 ):
     z = lax.axis_index("sp_0")
     y = lax.axis_index("sp_1")
     c = lax.axis_index("sp_2")
+    x = lax.axis_index("tp")
     sp = (z * 4 + y) * 2 + c
     nxt = lax.rem(sp + 1, 32)
     prv = lax.rem(sp + 31, 32)
+    left, right, across = lax.rem(x + 3, 4), lax.rem(x + 1, 4), lax.rem(x + 2, 4)
+    net = Net(send_sems, recv_sems)
 
     def at_sp(i):
         return {"sp_0": i // 8, "sp_1": lax.rem(i // 2, 4), "sp_2": lax.rem(i, 2)}
 
+    loads = [
+        pltpu.make_async_copy(src, dst, load_sems.at[i])
+        for i, (src, dst) in enumerate((
+            (sh_in, sh), (lh_in, lh), (ks_in, ks), (qs_in, qs),
+            (gate_in, weights.at[z, y, c, :, pl.ds(0, FF_DEV)]),
+            (up_in, weights.at[z, y, c, :, pl.ds(FF_DEV, FF_DEV)]),
+            (down_in, weights.at[z, y, c, :, DOWN_COLS]),
+            (so_in, projs.at[x, pl.ds(0, 256)]),
+            (lo_in, projs.at[x, pl.ds(256, 256)]),
+            (sg_in, sg), (lg_in, lg),
+            (residual.at[pl.ds(pl.multiple_of(x * OWN, OWN), OWN)], res),
+        ))
+    ]
+    for copy in loads:
+        copy.start()
+    loads_in, loads_own, loads_gate = loads[:4], loads[4:9], loads[9:]
+
     ypeers = [{"sp_1": lax.rem(y + d, 4)} for d in (1, 2, 3)]
     zpeers = [{"sp_0": lax.rem(z + d, 4)} for d in (1, 2, 3)]
+    xpeers = [{"tp": i} for i in (across, right, left)]
     sibling = {"sp_2": 1 - c}
     barrier = pltpu.get_barrier_semaphore()
-    peers = [at_sp(nxt), at_sp(prv), sibling] + ypeers + zpeers
+    peers = [at_sp(nxt), at_sp(prv), sibling] + ypeers + zpeers + xpeers
     for peer in peers:
         pl.semaphore_signal(barrier, inc=1, device_id=peer, device_id_type=MESH)
     pl.semaphore_wait(barrier, len(peers))
 
     sources = (sh, lh, ks, qs)
     halo_copies = [
-        pltpu.make_async_remote_copy(
-            src_ref=src.at[pl.ds(ROWS - 16, 16)], dst_ref=halo.at[i],
-            send_sem=hs_sem.at[i], recv_sem=hr_sem.at[i],
-            device_id=at_sp(nxt), device_id_type=MESH,
-        )
-        for i, src in enumerate(sources)
+        net.copy(src.at[pl.ds(ROWS - 16, 16)], halo.at[i], at_sp(nxt)) for i, src in enumerate((sh_in, lh_in, ks_in, qs_in))
     ]
     for copy in halo_copies:
         copy.start()
 
-    dtt[...] = jnp.zeros_like(dtt)
-    dtt[0:4, :] = jax.nn.softplus(sst[...])
-    dtt[4:6, :] = jax.nn.softplus(lst[...])
+    def span(part, size):
+        return pl.ds(0, size) if part is None else pl.ds(part * (size // 2), size // 2)
+
+    def y_first(cols):
+        return lambda i, p=None: weights.at[z, i, c, span(p, 32), cols]
+
+    def z_first(cols):
+        return lambda i, p=None: weights.at[i, y, c, pl.ds(32, 32) if p is None else pl.ds(32 + 16 * p, 16), cols]
+
+    def z_view(cols):
+        return lambda i, p=None: weights.at[i, span(p, 4), c, pl.ds(0, 32), cols]
+
+    def y_view(cols):
+        return lambda i, p=None: weights.at[span(p, 4), i, c, pl.ds(32, 32), cols]
+
+    def proj_view(i, p=None):
+        size = 256 if p is None else 128
+        return projs.at[i, pl.ds(pl.multiple_of(c * 256 + (0 if p is None else p * 128), 128), size)]
+
+    for copy in loads_own:
+        copy.wait()
+    first_rings = [
+        Ring(net, axis, at, view(cols))
+        for cols in (UP_COLS, DOWN_COLS)
+        for axis, at, view in (("sp_1", y, y_first), ("sp_0", z, z_first))
+    ]
+    proj = Ring(net, "tp", x, proj_view)
+    for ring in first_rings + [proj]:
+        ring.start()
+
+    dtt[...] = jax.nn.softplus(steps[...])
     ct[...] = jnp.zeros_like(ct)
     for h in range(6):
         d = sdec[h] if h < 4 else ldec[h - 4]
@@ -108,14 +209,14 @@
 
     lax.fori_loop(0, NBLK, sums, 0)
 
-    taps = (stap, ltap, ktap, qtap)
+    taps = [params[3:7, i * 256 : i * 256 + 256] for i in range(4)]
     dests = (xs, xl, kc, qc)
 
     def conv_of(ext, tap):
         acc = jnp.zeros((BLOCK, 256), F32)
         for k in range(4):
             shifted = ext if k == 3 else pltpu.roll(ext, 3 - k, 0)
-            acc = acc + tap[k : k + 1, :].astype(F32) * shifted[16:, :]
+            acc = acc + tap[k : k + 1, :] * shifted[16:, :]
         return silu(acc).astype(BF16)
 
     def conv_block(b, _):
@@ -125,6 +226,8 @@
             dst[block_rows(b), :] = conv_of(ext, tap)
         return 0
 
+    for copy in loads_in:
+        copy.wait()
     lax.fori_loop(1, NBLK, conv_block, 0)
     for copy in halo_copies:
         copy.wait()
@@ -133,6 +236,9 @@
         before = halo[i].astype(F32) * keep
         ext = jnp.concatenate([before, src[0:BLOCK, :].astype(F32)], axis=0)
         dst[0:BLOCK, :] = conv_of(ext, tap)
+
+    for ring in first_rings:
+        ring.forward()
 
     mine[...] = jnp.zeros_like(mine)
     mine_tot[...] = jnp.zeros_like(mine_tot)
@@ -160,13 +266,7 @@
     lax.fori_loop(0, NBLK, states, 0)
 
     sbuf[...] = mine[...].astype(BF16)
-    r1 = [
-        pltpu.make_async_remote_copy(
-            src_ref=src, dst_ref=dst, send_sem=s1_sem.at[i], recv_sem=r1_sem.at[i],
-            device_id=sibling, device_id_type=MESH,
-        )
-        for i, (src, dst) in enumerate(((sbuf, sib), (mine_tot, sib_tot)))
-    ]
+    r1 = [net.copy(sbuf, sib, sibling), net.copy(mine_tot, sib_tot, sibling)]
     for copy in r1:
         copy.start()
 
@@ -174,20 +274,20 @@
         rows = block_rows(b)
         cb = ccol[rows, :]
         parts = []
-        for g, x in ((0, xs), (1, xl)):
+        for g, vals in ((0, xs), (1, xl)):
             lanes = slice(g * 128, g * 128 + 128)
             scores = dot(qc[rows, lanes], kc[rows, lanes], ((1,), (1,)))
-            heads = []
+            found = []
             for h in range(4) if g == 0 else range(4, 6):
                 gap = jnp.broadcast_to(cb[:, h : h + 1], (BLOCK, BLOCK)) - ct[h : h + 1, rows]
                 decay = jnp.exp(jnp.where(causal, gap, -1e30))
                 w = (scores * decay * dtt[h : h + 1, rows]).astype(BF16)
                 at = (h // 2 if g == 0 else h - 4) * 128
-                heads.append(dot(w, x[rows, at : at + 128]))
+                found.append(dot(w, vals[rows, at : at + 128]))
             if g == 0:
-                parts += [jnp.where(low, heads[0], heads[1]), jnp.where(low, heads[2], heads[3])]
+                parts += [jnp.where(low, found[0], found[1]), jnp.where(low, found[2], found[3])]
             else:
-                parts += heads
+                parts += found
         inside[rows, :] = jnp.concatenate(parts, axis=1)
         return 0
 
@@ -208,18 +308,14 @@
     chip_tot = t_me + t_sib
     ysend[...] = chip.astype(BF16)
     ytot_send[...] = chip_tot
-    def peer_copies(send, tot_send, rec, tot_rec, sems, peers_):
-        ss, rs = sems
+
+    def peer_copies(send, tot_send, rec, tot_rec, peers_):
         made = []
         for i, peer in enumerate(peers_):
-            for j, (src, dst) in enumerate(((send, rec.at[i]), (tot_send, tot_rec.at[i]))):
-                made.append(pltpu.make_async_remote_copy(
-                    src_ref=src, dst_ref=dst, send_sem=ss.at[2 * i + j], recv_sem=rs.at[2 * i + j],
-                    device_id=peer, device_id_type=MESH,
-                ))
+            made += [net.copy(send, rec.at[i], peer), net.copy(tot_send, tot_rec.at[i], peer)]
         return made
 
-    r2 = peer_copies(ysend, ytot_send, yrec, ytot, (ys_sem, yr_sem), ypeers)
+    r2 = peer_copies(ysend, ytot_send, yrec, ytot, ypeers)
     for copy in r2:
         copy.start()
     lax.fori_loop(2, 5, intra, 0)
@@ -244,19 +340,32 @@
         plane_tot = jnp.where(valid, plane_tot + ytot[3 - e], plane_tot)
     zsend[...] = plane.astype(BF16)
     ztot_send[...] = plane_tot
-    r3 = peer_copies(zsend, ztot_send, zrec, ztot, (zs_sem, zr_sem), zpeers)
+    r3 = peer_copies(zsend, ztot_send, zrec, ztot, zpeers)
     for copy in r3:
         copy.start()
+    for ring in first_rings:
+        ring.finish()
+    second_rings = [
+        Ring(net, axis, at, view(cols))
+        for cols in (UP_COLS, DOWN_COLS)
+        for axis, at, view in (("sp_0", z, z_view), ("sp_1", y, y_view))
+    ]
+    for ring in second_rings:
+        ring.start()
+    shared = [
+        [net.copy(z_view(cols)(z), z_view(cols)(z), sibling), net.copy(y_view(cols)(y), y_view(cols)(y), sibling)]
+        for cols in (UP_COLS, DOWN_COLS)
+    ]
+    for group in shared:
+        for copy in group:
+            copy.start()
     lax.fori_loop(5, NBLK, intra, 0)
     for copy in r3:
         copy.wait()
     ez, _ = before_of(z, zrec, ztot)
     entering = ez * jnp.exp(ty)[0:1, :] + ey
     esend[...] = entering
-    r4 = pltpu.make_async_remote_copy(
-        src_ref=esend, dst_ref=ebuf.at[half], send_sem=s4_sem, recv_sem=r4_sem,
-        device_id=sibling, device_id_type=MESH,
-    )
+    r4 = net.copy(esend, ebuf.at[half], sibling)
     r4.start()
     r4.wait()
     own = esend[...]
@@ -268,6 +377,13 @@
     second = enter * jnp.exp(t_sib)[0:1, :] + sib[...].astype(F32)
     mine[...] = jnp.where(first, enter, second)
 
+    proj.forward()
+    shared_proj = [net.copy(proj_view(i), proj_view(i), sibling) for i in (x, left, right)]
+    for copy in shared_proj:
+        copy.start()
+    for copy in loads_gate:
+        copy.wait()
+
     def finish(b, _):
         rows = block_rows(b)
         state = (hloc[b] + eoff[b][0:1, :] * mine[...]).astype(BF16)
@@ -276,7 +392,6 @@
         for i in range(4):
             g, at = i // 2, (i % 2) * 128
             gate_ref = sg if g == 0 else lg
-            gain_ref = sgain if g == 0 else lgain
             v = inside[rows, i * 128 : i * 128 + 128] + carried[g][:, at : at + 128] * grow[i]
             v = v * silu(gate_ref[rows, at : at + 128].astype(F32))
             sq = v * v
@@ -286,26 +401,157 @@
                 inv = jnp.where(low, lax.rsqrt(s0 / 64 + EPS), lax.rsqrt(s1 / 64 + EPS))
             else:
                 inv = lax.rsqrt(jnp.sum(sq, axis=1, keepdims=True) / 128 + EPS)
-            v = v * inv * gain_ref[:, at : at + 128].astype(F32)
-            out[rows, i * 128 : i * 128 + 128] = v.astype(BF16)
-        return 0
-
-    lax.fori_loop(0, NBLK, finish, 0)
-
-
-def ssm(*operands):
+            v = v * inv * params[7:8, i * 128 : i * 128 + 128]
+            heads[rows, i * 128 : i * 128 + 128] = v.astype(BF16)
+        return 0
+
+
+    exchange = []
+    for peer in (across, right, left, x):
+        for b in range(2):
+            finish(peer * 2 + b, 0)
+        rows = pl.ds(pl.multiple_of(peer * OWN, OWN), OWN)
+        if peer is not x:
+            exchange.append(net.copy(heads.at[rows], chans.at[x], {"tp": peer}))
+            exchange[-1].start()
+    own_rows = pl.ds(pl.multiple_of(x * OWN, OWN), OWN)
+    chans[x] = heads[own_rows, :]
+
+    def share(copies):
+        for copy in copies:
+            copy.start()
+        return copies
+
+    def share_arrived(k, which):
+        zr, yr = second_rings[2 * k], second_rings[2 * k + 1]
+        cols = (UP_COLS, DOWN_COLS)[k]
+        zs = [zr.before, zr.after] if which == 0 else [lax.rem(z + 2, 4)]
+        ys = [yr.before, yr.after] if which == 0 else [lax.rem(y + 2, 4)]
+        return share(
+            [net.copy(z_view(cols)(i), z_view(cols)(i), sibling) for i in zs]
+            + [net.copy(y_view(cols)(i), y_view(cols)(i), sibling) for i in ys]
+        )
+
+    proj.finish()
+    shared_proj += share([net.copy(proj_view(across), proj_view(across), sibling)])
+    for k in (0, 1):
+        second_rings[2 * k].forward()
+        second_rings[2 * k + 1].forward()
+        shared[k] += share_arrived(k, 0)
+    for copy in shared_proj + exchange:
+        copy.wait()
+
+    def project(n, _):
+        cols = pl.ds(pl.multiple_of(n * 256, 256), 256)
+        acc = dot(chans[0], projs[0, :, cols])
+        for i in range(1, 4):
+            acc = acc + dot(chans[i], projs[i, :, cols])
+        mixed[:, cols] = acc
+        return 0
+
+    lax.fori_loop(0, 8, project, 0)
+
+    def norms(r, _):
+        rows = pl.ds(pl.multiple_of(r * 32, 32), 32)
+        v = mixed[rows, :]
+        v = v * lax.rsqrt(jnp.mean(v * v, axis=1, keepdims=True) + EPS)
+        v = res[rows, :].astype(F32) + v * params[0:1, :]
+        mixed[rows, :] = v
+        v = v * lax.rsqrt(jnp.mean(v * v, axis=1, keepdims=True) + EPS)
+        rows_in[x, rows, :] = (v * params[1:2, :]).astype(BF16)
+        return 0
+
+    lax.fori_loop(0, OWN // 32, norms, 0)
+
+    gather = Ring(net, "tp", x, lambda i, p: rows_in.at[i, pl.ds(p * 128, 128)], (0, 1))
+    gather.start()
+
+    def wait_weights(k):
+        second_rings[2 * k].finish()
+        second_rings[2 * k + 1].finish()
+        for copy in shared[k] + share_arrived(k, 1):
+            copy.wait()
+
+    def gate_up(i):
+        def tile(n, _):
+            g_cols = pl.ds(pl.multiple_of(n * 128, 128), 128)
+            u_cols = pl.ds(pl.multiple_of(FF_DEV + n * 128, 128), 128)
+            w = jnp.concatenate(
+                [weights[:, :, :, :, g_cols].reshape(2048, 128), weights[:, :, :, :, u_cols].reshape(2048, 128)], axis=1
+            )
+            both = dot(rows_in[i], w)
+            hidden[:, g_cols] = (silu(both[:, :128]) * both[:, 128:]).astype(BF16)
+            return 0
+
+        lax.fori_loop(0, FF_DEV // 128, tile, 0)
+
+    def down(i):
+        def tile(n, _):
+            w = weights[n // 2, pl.ds(lax.rem(n, 2) * 2, 2), :, :, DOWN_COLS].reshape(256, FF_DEV)
+            parts_out[i, :, pl.ds(pl.multiple_of(n * 256, 256), 256)] = dot(hidden[...], w, ((1,), (1,))).astype(BF16)
+            return 0
+
+        lax.fori_loop(0, 8, tile, 0)
+
+    h0, h1 = pl.ds(0, 128), pl.ds(128, 128)
+    to_left, to_right = {"tp": left}, {"tp": right}
+    wait_weights(0)
+    gate_up(x)
+    wait_weights(1)
+    down(x)
+    gather.forward()
+    gather.neighbours()
+    gate_up(left)
+    down(left)
+    sends = [net.copy(parts_out.at[left, h0], from_right.at[h0], to_left)]
+    sends[-1].start()
+    gate_up(right)
+    down(right)
+    sends.append(net.copy(parts_out.at[right, h1], from_left.at[h1], to_right))
+    sends[-1].start()
+    gather.finish()
+    gate_up(across)
+    down(across)
+    relays = share([
+        net.copy(parts_out.at[across, h0], relay.at[0], to_right),
+        net.copy(parts_out.at[across, h1], relay.at[1], to_left),
+    ])
+    for k, (peer, rows, dst, to) in enumerate(((right, h0, from_left, to_right), (left, h1, from_right, to_left))):
+        relays[k].wait_recv()
+        relay_sum[k] = (parts_out[peer, rows, :].astype(F32) + relay[k].astype(F32)).astype(BF16)
+        sends.append(net.copy(relay_sum.at[k], dst.at[rows], to))
+        sends[-1].start()
+    for copy in relays:
+        copy.wait_send()
+    for copy in sends:
+        copy.wait()
+
+    def last(r, _):
+        rows = pl.ds(pl.multiple_of(r * 32, 32), 32)
+        v = parts_out[x, rows, :].astype(F32) + from_left[rows, :].astype(F32) + from_right[rows, :].astype(F32)
+        v = v * lax.rsqrt(jnp.mean(v * v, axis=1, keepdims=True) + EPS)
+        out[rows, :] = (mixed[rows, :] + 0.5 * v * params[2:3, :]).astype(BF16)
+        return 0
+
+    lax.fori_loop(0, OWN // 32, last, 0)
+
+
+COPIES = 120
+
+
+def layer(*operands):
     vm = pl.BlockSpec(memory_space=pltpu.VMEM)
     sm = pl.BlockSpec(memory_space=pltpu.SMEM)
+    hbm = pl.BlockSpec(memory_space=pl.ANY)
     dma = pltpu.SemaphoreType.DMA
-    rows_bf = pltpu.VMEM((ROWS, 256), BF16)
+    chan = pltpu.VMEM((ROWS, 256), BF16)
     return pl.pallas_call(
-        ssm_kernel,
-        name="ssm",
-        out_shape=jax.ShapeDtypeStruct((ROWS, 512), BF16),
-        in_specs=[vm] * 12 + [sm] * 2 + [vm] * 2,
+        layer_kernel,
+        name="layer",
+        out_shape=jax.ShapeDtypeStruct((OWN, 2048), BF16),
+        in_specs=[hbm] * 12 + [vm] * 2 + [sm] * 2,
         out_specs=vm,
-        scratch_shapes=[
-            rows_bf, rows_bf, rows_bf, rows_bf,
+        scratch_shapes=[chan] * 10 + [
             pltpu.VMEM((8, ROWS), F32), pltpu.VMEM((8, ROWS), F32),
             pltpu.VMEM((ROWS, 128), F32), pltpu.VMEM((ROWS, 128), F32),
             pltpu.VMEM((NBLK, 128, 512), F32), pltpu.VMEM((NBLK, 8, 512), F32),
@@ -318,15 +564,20 @@
             pltpu.VMEM((64, 512), BF16), pltpu.VMEM((8, 512), F32),
             pltpu.VMEM((3, 64, 512), BF16), pltpu.VMEM((3, 8, 512), F32),
             pltpu.VMEM((64, 512), F32), pltpu.VMEM((128, 512), F32),
-            dma((4,)), dma((4,)), dma((2,)), dma((2,)), dma((6,)), dma((6,)), dma((6,)), dma((6,)), dma, dma,
+            pltpu.VMEM((ROWS, 512), BF16), pltpu.VMEM((4, OWN, 512), BF16),
+            pltpu.VMEM((4, 4, 2, 64, 3 * FF_DEV), BF16), pltpu.VMEM((4, 512, 2048), BF16),
+            pltpu.VMEM((OWN, 2048), BF16), pltpu.VMEM((OWN, 2048), F32),
+            pltpu.VMEM((4, OWN, 2048), BF16), pltpu.VMEM((OWN, FF_DEV), BF16),
+            pltpu.VMEM((4, OWN, 2048), BF16),
+            pltpu.VMEM((2, 128, 2048), BF16), pltpu.VMEM((2, 128, 2048), BF16),
+            pltpu.VMEM((OWN, 2048), BF16), pltpu.VMEM((OWN, 2048), BF16),
+            dma((COPIES,)), dma((COPIES,)), dma((12,)),
         ],
-        compiler_params=pltpu.CompilerParams(collective_id=0, has_side_effects=True, vmem_limit_bytes=48 * 1024 * 1024),
-        cost_estimate=pl.CostEstimate(flops=4_000_000_000, bytes_accessed=5_000_000, transcendentals=0),
+        compiler_params=pltpu.CompilerParams(
+            collective_id=0, has_side_effects=True, vmem_limit_bytes=67043328
+        ),
+        cost_estimate=pl.CostEstimate(flops=22_000_000_000, bytes_accessed=30_000_000, transcendentals=0),
     )(*operands)
-
-
-def unit_rms(values):
-    return values * lax.rsqrt(jnp.mean(values * values, axis=-1, keepdims=True) + EPS)
 
 
 def local(
@@ -335,36 +586,21 @@
     small_gain, large_gain, small_out, large_out, mixer_gain, ffn_in_gain,
     gate_proj, up_proj, down_proj, ffn_out_gain,
 ):
-    length = residual.shape[0]
-    weights = lax.all_gather(
-        jnp.concatenate([gate_proj, up_proj, down_proj], axis=1), SP, axis=0, tiled=True
+    taps = jnp.concatenate([small_taps, large_taps, key_taps.reshape(4, 256), query_taps.reshape(4, 256)], axis=1)
+    head_gain = jnp.concatenate([small_gain, large_gain]).reshape(1, 512)
+    params = jnp.concatenate(
+        [
+            jnp.stack([mixer_gain, ffn_in_gain, ffn_out_gain]),
+            jnp.pad(taps, ((0, 0), (0, 1024))),
+            jnp.pad(head_gain, ((0, 0), (0, 1536))),
+        ]
+    ).astype(F32)
+    steps = jnp.concatenate([small_step.T, large_step.T, jnp.zeros((2, ROWS), F32)])
+    return layer(
+        residual, small_heads, large_heads, state_keys.reshape(ROWS, 256), state_queries.reshape(ROWS, 256),
+        small_gate, large_gate, gate_proj, up_proj, down_proj, small_out, large_out,
+        steps, params, small_decay, large_decay,
     )
-    ff = gate_proj.shape[1]
-    normed = ssm(
-        small_heads, large_heads, state_keys.reshape(length, 256), state_queries.reshape(length, 256),
-        small_gate, large_gate, small_step.T, large_step.T, small_taps, large_taps,
-        key_taps.reshape(4, 256), query_taps.reshape(4, 256), small_decay, large_decay,
-        small_gain.reshape(1, 256), large_gain.reshape(1, 256),
-    )
-    partial_value = jnp.dot(normed[:, :256], small_out, preferred_element_type=F32)
-    partial_value = partial_value + jnp.dot(normed[:, 256:], large_out, preferred_element_type=F32)
-    mix = lax.psum_scatter(partial_value.astype(BF16), "tp", scatter_dimension=0, tiled=True).astype(F32)
-    share = length // lax.axis_size("tp")
-    own = lax.dynamic_slice_in_dim(residual, lax.axis_index("tp") * share, share, 0).astype(F32)
-    mixed = own + unit_rms(mix) * mixer_gain.astype(F32)
-    normed_in = (unit_rms(mixed) * ffn_in_gain.astype(F32)).astype(BF16)
-    normed_in = lax.all_gather(normed_in, "tp", axis=0, tiled=True)
-    gate = jnp.dot(normed_in, weights[:, :ff], preferred_element_type=F32)
-    up_values = jnp.dot(normed_in, weights[:, ff : 2 * ff], preferred_element_type=F32)
-    hidden = (jax.nn.silu(gate) * up_values).astype(BF16)
-    ffn = lax.psum_scatter(
-        lax.dot_general(
-            hidden, weights[:, 2 * ff :], (((1,), (1,)), ((), ())), preferred_element_type=F32
-        ).astype(BF16),
-        "tp", scatter_dimension=0, tiled=True,
-    ).astype(F32)
-    updated = mixed + 0.5 * unit_rms(ffn) * ffn_out_gain.astype(F32)
-    return updated.astype(BF16)
 
 
 def solution(mesh):

time: 326 us -> 160 us (0.49)
  waiting for transfers between devices: 214 us -> 0 us
  Pallas kernels: 33.3 us -> 148 us
  matrix products: 38.8 us -> 0 us
  between operations: 13.3 us -> 0.02 us
  other arithmetic: 12.4 us -> 3.41 us
  local copies, waits for them, and re-layouts: 13 us -> 7.59 us
    all_gather x2 -> x0, waiting for transfers between devices: 124 us -> none  [the longest x1 77.2 us: local(): lax.all_gather(jnp.concatenate([gate_proj, up_proj, down_proj], axis=1),...]
    pallas_call x1, Pallas kernels: 33.3 us -> 148 us  [layer(): pl.pallas_call(layer_kernel, name='layer', out_shape=jax.ShapeDtypeStruct...]
    reduce_scatter x2 -> x0, waiting for transfers between devices: 90.3 us -> none  [the longest x1 45.2 us: local(): lax.psum_scatter(lax.dot_general(hidden, weights[:, 2 * ff:], (((1,), (1,...]
    dot_general x4 -> x0, matrix products: 38.8 us -> none  [the longest x1 22.7 us: local(): lax.dot_general(hidden, weights[:, 2 * ff:], (((1,), (1,)), ((), ())), pr...]
    unnamed x38 -> x1, local copies, waits for them, and re-layouts: 9.53 us -> 2.3 us
    convert_element_type x4 -> x1, other arithmetic: 6.4 us -> 0.62 us  [local(): params = jnp.concatenate([jnp.stack([mixer_gain, ffn_in_gain, ffn_out_gai...]
    reduce_sum x3 -> x0, other arithmetic: 5.18 us -> none  [unit_rms(): jnp.mean(values * values, axis=-1, keepdims=True) + EPS]
  transfers between devices with their start and end apart: 4 -> 0, of which waited for: 4 -> 0; matrix products, arithmetic and copies ran while one was open for 0% -> 0% of each run, Pallas kernels for 0% -> 0%
where the time goes in v2:
time: 160 us; the launch traced here: 159 us
  Pallas kernels  148 us (92%)
  local copies, waits for them, and re-layouts  7.59 us (5%)
  other arithmetic  3.41 us (2%)
    pallas_call x1, Pallas kernels, layer(): pl.pallas_call(layer_kernel, name='layer', out_shape=jax.ShapeDtypeStruct...  148 us

profile of v2, /device:TPU:1, one launch (start us, length us, event | category | flops | bytes accessed | tf_op | source)
XLA Modules:
  0.0 158.6 jit_solution(11485882027398528894)
XLA Ops:
  0.0 0.1 pad.18.clone
  0.1 0.7 pad_maximum_fusion
  0.8 0.7 copy_bitcast_fusion.2
  1.5 0.7 stack.9
  2.2 0.7 stack.10
  2.9 0.7 stack.11
  3.6 0.7 fusion.6
  4.3 0.1 concatenate.15
  4.3 1.4 maximum_maximum_fusion.steps
  5.7 0.6 convert_element_type.7.params
  6.4 2.3 %copy_bitcast_fusion = (bf16[1024,256]{1,0:T(8,128)(2,1)}, bf16[1024,256]{1,0:T(8,128)(2,1)}) fusion(bf16[128,8,2,128]{3,2,1,0:T(2,128)(2,1)} %bitcast.14, bf16[128,8,2,128]{3,2,1,0:T(2,128)(2,1)} %bitcast.15), kind=kLoop, calls=%fused_computation | loop fusion | bytes 2097152 | tf_op jit(solution)/shard_map/reshape | solution.py:600
  8.7 147.6 %layer.1 = bf16[256,2048]{1,0:T(8,128)(2,1)} custom-call(bf16[1024,2048]{1,0:T(8,128)(2,1)} %residual.1, bf16[1024,256]{1,0:T(8,128)(2,1)} %sh_in.1, bf16[1024,256]{1,0:T(8,128)(2,1)} %lh_in.1, bf16[1024,256]{1,0:T(8,128)(2,1)} %get-tuple-element.8.ks_in, bf16[1024,256]{1,0:T(8,128)(2,1)} %get-tuple-element.7.qs_in, bf16[1024,256]{1,0:T(8,128)(2,1)} %sg_in.1, ...), custom_call_target="tpu_custom_call" | custom-call | flops 22000001024 | bytes 30000000 | tf_op jit(solution)/shard_map/layer/pallas_call | solution.py:548
  156.3 2.3 %copy.35 = bf16[256,2048]{1,0:T(8,128)(2,1)} copy(bf16[256,2048]{1,0:T(8,128)(2,1)} %layer.1) | data formatting | bytes 2097152
  (3 shorter events, 0.0 us)

commit v3 on v2

--- a/solution.py
+++ b/solution.py
@@ -46,6 +46,8 @@
 
 
 OWN = 256
+STEPS = 4
+PART = OWN // STEPS
 FF_DEV = 1408
 UP_COLS = pl.ds(0, 2 * FF_DEV)
 DOWN_COLS = pl.ds(2 * FF_DEV, FF_DEV)
@@ -101,12 +103,12 @@
 
 def layer_kernel(
     residual, sh_in, lh_in, ks_in, qs_in, sg_in, lg_in, gate_in, up_in, down_in, so_in, lo_in,
-    steps, params, sdec, ldec,
+    small_steps, large_steps, params, sdec, ldec,
     out,
-    sh, lh, ks, qs, sg, lg,
-    xs, xl, kc, qc, dtt, ct, ccol, dcol, hloc, eoff, inside,
+    xs, xl, kc, qc, sg, lg,
+    dtt, ct, ccol, dcol, hloc, eoff, inside,
     halo, mine, mine_tot, sbuf, sib, sib_tot, ysend, ytot_send, yrec, ytot, zsend, ztot_send, zrec, ztot, esend, ebuf,
-    heads, chans, weights, projs, res, mixed, rows_in, hidden, parts_out, relay, relay_sum, from_left, from_right,
+    chans, weights, projs, res, mix, mixed, rows_in, hidden, parts_out, relay, relay_sum, from_left, from_right,
     send_sems, recv_sems, load_sems,
 ):
     z = lax.axis_index("sp_0")
@@ -125,14 +127,14 @@
     loads = [
         pltpu.make_async_copy(src, dst, load_sems.at[i])
         for i, (src, dst) in enumerate((
-            (sh_in, sh), (lh_in, lh), (ks_in, ks), (qs_in, qs),
+            (sh_in, xs), (lh_in, xl), (ks_in, kc), (qs_in, qc),
             (gate_in, weights.at[z, y, c, :, pl.ds(0, FF_DEV)]),
             (up_in, weights.at[z, y, c, :, pl.ds(FF_DEV, FF_DEV)]),
             (down_in, weights.at[z, y, c, :, DOWN_COLS]),
             (so_in, projs.at[x, pl.ds(0, 256)]),
             (lo_in, projs.at[x, pl.ds(256, 256)]),
             (sg_in, sg), (lg_in, lg),
-            (residual.at[pl.ds(pl.multiple_of(x * OWN, OWN), OWN)], res),
+            (residual, res),
         ))
     ]
     for copy in loads:
@@ -149,7 +151,6 @@
         pl.semaphore_signal(barrier, inc=1, device_id=peer, device_id_type=MESH)
     pl.semaphore_wait(barrier, len(peers))
 
-    sources = (sh, lh, ks, qs)
     halo_copies = [
         net.copy(src.at[pl.ds(ROWS - 16, 16)], halo.at[i], at_sp(nxt)) for i, src in enumerate((sh_in, lh_in, ks_in, qs_in))
     ]
@@ -186,7 +187,9 @@
     for ring in first_rings + [proj]:
         ring.start()
 
-    dtt[...] = jax.nn.softplus(steps[...])
+    dtt[...] = jnp.zeros_like(dtt)
+    dtt[0:4, :] = jax.nn.softplus(small_steps[...])
+    dtt[4:6, :] = jax.nn.softplus(large_steps[...])
     ct[...] = jnp.zeros_like(ct)
     for h in range(6):
         d = sdec[h] if h < 4 else ldec[h - 4]
@@ -196,6 +199,7 @@
     tc = lax.broadcasted_iota(jnp.int32, (BLOCK, BLOCK), 1)
     upper = (tr <= tc).astype(F32)
     low = tc < 64
+    low_part = low[:PART]
     causal = tc <= tr
 
     def sums(b, _):
@@ -210,7 +214,7 @@
     lax.fori_loop(0, NBLK, sums, 0)
 
     taps = [params[3:7, i * 256 : i * 256 + 256] for i in range(4)]
-    dests = (xs, xl, kc, qc)
+    keep = jnp.where(sp == 0, 0.0, 1.0)
 
     def conv_of(ext, tap):
         acc = jnp.zeros((BLOCK, 256), F32)
@@ -219,24 +223,26 @@
             acc = acc + tap[k : k + 1, :] * shifted[16:, :]
         return silu(acc).astype(BF16)
 
-    def conv_block(b, _):
-        start = pl.multiple_of(b * BLOCK - 16, 16)
-        for src, tap, dst in zip(sources, taps, dests):
-            ext = src[pl.ds(start, BLOCK + 16), :].astype(F32)
-            dst[block_rows(b), :] = conv_of(ext, tap)
-        return 0
+    def convolve(which):
+        refs = (xs, xl, kc, qc)
+
+        def conv_block(i, _):
+            b = NBLK - 1 - i
+            start = pl.multiple_of(b * BLOCK - 16, 16)
+            for k in which:
+                refs[k][block_rows(b), :] = conv_of(refs[k][pl.ds(start, BLOCK + 16), :].astype(F32), taps[k])
+            return 0
+
+        lax.fori_loop(0, NBLK - 1, conv_block, 0)
+        for k in which:
+            halo_copies[k].wait()
+        for k in which:
+            ext = jnp.concatenate([halo[k].astype(F32) * keep, refs[k][0:BLOCK, :].astype(F32)], axis=0)
+            refs[k][0:BLOCK, :] = conv_of(ext, taps[k])
 
     for copy in loads_in:
         copy.wait()
-    lax.fori_loop(1, NBLK, conv_block, 0)
-    for copy in halo_copies:
-        copy.wait()
-    keep = jnp.where(sp == 0, 0.0, 1.0)
-    for i, (src, tap, dst) in enumerate(zip(sources, taps, dests)):
-        before = halo[i].astype(F32) * keep
-        ext = jnp.concatenate([before, src[0:BLOCK, :].astype(F32)], axis=0)
-        dst[0:BLOCK, :] = conv_of(ext, tap)
-
+    convolve((0, 1, 2))
     for ring in first_rings:
         ring.forward()
 
@@ -269,6 +275,7 @@
     r1 = [net.copy(sbuf, sib, sibling), net.copy(mine_tot, sib_tot, sibling)]
     for copy in r1:
         copy.start()
+    convolve((3,))
 
     def intra(b, _):
         rows = block_rows(b)
@@ -291,7 +298,6 @@
         inside[rows, :] = jnp.concatenate(parts, axis=1)
         return 0
 
-    lax.fori_loop(0, 2, intra, 0)
     for copy in r1:
         copy.wait()
 
@@ -318,7 +324,7 @@
     r2 = peer_copies(ysend, ytot_send, yrec, ytot, ypeers)
     for copy in r2:
         copy.start()
-    lax.fori_loop(2, 5, intra, 0)
+    lax.fori_loop(0, 4, intra, 0)
     for copy in r2:
         copy.wait()
 
@@ -359,7 +365,7 @@
     for group in shared:
         for copy in group:
             copy.start()
-    lax.fori_loop(5, NBLK, intra, 0)
+    lax.fori_loop(4, NBLK, intra, 0)
     for copy in r3:
         copy.wait()
     ez, _ = before_of(z, zrec, ztot)
@@ -384,8 +390,14 @@
     for copy in loads_gate:
         copy.wait()
 
-    def finish(b, _):
-        rows = block_rows(b)
+    def share(copies):
+        for copy in copies:
+            copy.start()
+        return copies
+
+    def finish(s, j):
+        b = 2 * j + s // 2
+        rows = pl.ds(pl.multiple_of(j * OWN + s * PART, PART), PART)
         state = (hloc[b] + eoff[b][0:1, :] * mine[...]).astype(BF16)
         grow = spread(jnp.exp(ccol[rows, :]))
         carried = [dot(qc[rows, g * 128 : g * 128 + 128], state[:, g * 256 : g * 256 + 256]) for g in (0, 1)]
@@ -396,31 +408,22 @@
             v = v * silu(gate_ref[rows, at : at + 128].astype(F32))
             sq = v * v
             if g == 0:
-                s0 = jnp.sum(jnp.where(low, sq, 0.0), axis=1, keepdims=True)
-                s1 = jnp.sum(jnp.where(low, 0.0, sq), axis=1, keepdims=True)
-                inv = jnp.where(low, lax.rsqrt(s0 / 64 + EPS), lax.rsqrt(s1 / 64 + EPS))
+                s0 = jnp.sum(jnp.where(low_part, sq, 0.0), axis=1, keepdims=True)
+                s1 = jnp.sum(jnp.where(low_part, 0.0, sq), axis=1, keepdims=True)
+                inv = jnp.where(low_part, lax.rsqrt(s0 / 64 + EPS), lax.rsqrt(s1 / 64 + EPS))
             else:
                 inv = lax.rsqrt(jnp.sum(sq, axis=1, keepdims=True) / 128 + EPS)
             v = v * inv * params[7:8, i * 128 : i * 128 + 128]
-            heads[rows, i * 128 : i * 128 + 128] = v.astype(BF16)
+            chans[x, s, pl.ds(pl.multiple_of(j * PART, PART), PART), i * 128 : i * 128 + 128] = v.astype(BF16)
         return 0
 
 
-    exchange = []
-    for peer in (across, right, left, x):
-        for b in range(2):
-            finish(peer * 2 + b, 0)
-        rows = pl.ds(pl.multiple_of(peer * OWN, OWN), OWN)
-        if peer is not x:
-            exchange.append(net.copy(heads.at[rows], chans.at[x], {"tp": peer}))
-            exchange[-1].start()
-    own_rows = pl.ds(pl.multiple_of(x * OWN, OWN), OWN)
-    chans[x] = heads[own_rows, :]
-
-    def share(copies):
-        for copy in copies:
-            copy.start()
-        return copies
+    gathers = [
+        Ring(net, "tp", x, lambda i, p, s=s: chans.at[i, s, pl.ds(p * 128, 128)], (0, 1)) for s in range(STEPS)
+    ]
+
+    def finish_step(s):
+        lax.fori_loop(0, 4, lambda j, _: finish(s, j), 0)
 
     def share_arrived(k, which):
         zr, yr = second_rings[2 * k], second_rings[2 * k + 1]
@@ -432,39 +435,10 @@
             + [net.copy(y_view(cols)(i), y_view(cols)(i), sibling) for i in ys]
         )
 
-    proj.finish()
-    shared_proj += share([net.copy(proj_view(across), proj_view(across), sibling)])
-    for k in (0, 1):
+    def forward_weights(k):
         second_rings[2 * k].forward()
         second_rings[2 * k + 1].forward()
         shared[k] += share_arrived(k, 0)
-    for copy in shared_proj + exchange:
-        copy.wait()
-
-    def project(n, _):
-        cols = pl.ds(pl.multiple_of(n * 256, 256), 256)
-        acc = dot(chans[0], projs[0, :, cols])
-        for i in range(1, 4):
-            acc = acc + dot(chans[i], projs[i, :, cols])
-        mixed[:, cols] = acc
-        return 0
-
-    lax.fori_loop(0, 8, project, 0)
-
-    def norms(r, _):
-        rows = pl.ds(pl.multiple_of(r * 32, 32), 32)
-        v = mixed[rows, :]
-        v = v * lax.rsqrt(jnp.mean(v * v, axis=1, keepdims=True) + EPS)
-        v = res[rows, :].astype(F32) + v * params[0:1, :]
-        mixed[rows, :] = v
-        v = v * lax.rsqrt(jnp.mean(v * v, axis=1, keepdims=True) + EPS)
-        rows_in[x, rows, :] = (v * params[1:2, :]).astype(BF16)
-        return 0
-
-    lax.fori_loop(0, OWN // 32, norms, 0)
-
-    gather = Ring(net, "tp", x, lambda i, p: rows_in.at[i, pl.ds(p * 128, 128)], (0, 1))
-    gather.start()
 
     def wait_weights(k):
         second_rings[2 * k].finish()
@@ -472,71 +446,132 @@
         for copy in shared[k] + share_arrived(k, 1):
             copy.wait()
 
-    def gate_up(i):
+    def project(s):
+        def tile(n, _):
+            cols = pl.ds(pl.multiple_of(n * 256, 256), 256)
+            acc = dot(chans[0, s], projs[0, :, cols])
+            for i in range(1, 4):
+                acc = acc + dot(chans[i, s], projs[i, :, cols])
+            mix[:, cols] = acc
+            return 0
+
+        lax.fori_loop(0, 8, tile, 0)
+
+        def norms(r, _):
+            rows = pl.ds(pl.multiple_of(r * 32, 32), 32)
+            v = mix[rows, :]
+            v = v * lax.rsqrt(jnp.mean(v * v, axis=1, keepdims=True) + EPS)
+            at = (r // 2) * OWN + lax.rem(r, 2) * 32 + s * PART
+            v = res[pl.ds(pl.multiple_of(at, 32), 32), :].astype(F32) + v * params[0:1, :]
+            mix[rows, :] = v
+            v = v * lax.rsqrt(jnp.mean(v * v, axis=1, keepdims=True) + EPS)
+            rows_in[rows, :] = (v * params[1:2, :]).astype(BF16)
+            return 0
+
+        lax.fori_loop(0, OWN // 32, norms, 0)
+        mixed[s * PART : s * PART + PART, :] = mix[pl.ds(pl.multiple_of(x * PART, PART), PART), :]
+
+    def gate_up():
         def tile(n, _):
             g_cols = pl.ds(pl.multiple_of(n * 128, 128), 128)
             u_cols = pl.ds(pl.multiple_of(FF_DEV + n * 128, 128), 128)
             w = jnp.concatenate(
                 [weights[:, :, :, :, g_cols].reshape(2048, 128), weights[:, :, :, :, u_cols].reshape(2048, 128)], axis=1
             )
-            both = dot(rows_in[i], w)
+            both = dot(rows_in[...], w)
             hidden[:, g_cols] = (silu(both[:, :128]) * both[:, 128:]).astype(BF16)
             return 0
 
         lax.fori_loop(0, FF_DEV // 128, tile, 0)
 
-    def down(i):
+    def down(s):
         def tile(n, _):
             w = weights[n // 2, pl.ds(lax.rem(n, 2) * 2, 2), :, :, DOWN_COLS].reshape(256, FF_DEV)
-            parts_out[i, :, pl.ds(pl.multiple_of(n * 256, 256), 256)] = dot(hidden[...], w, ((1,), (1,))).astype(BF16)
+            part = dot(hidden[...], w, ((1,), (1,))).astype(BF16).reshape(4, PART, 256)
+            parts_out[:, s * PART : s * PART + PART, pl.ds(pl.multiple_of(n * 256, 256), 256)] = part
             return 0
 
         lax.fori_loop(0, 8, tile, 0)
 
-    h0, h1 = pl.ds(0, 128), pl.ds(128, 128)
     to_left, to_right = {"tp": left}, {"tp": right}
-    wait_weights(0)
-    gate_up(x)
-    wait_weights(1)
-    down(x)
-    gather.forward()
-    gather.neighbours()
-    gate_up(left)
-    down(left)
-    sends = [net.copy(parts_out.at[left, h0], from_right.at[h0], to_left)]
-    sends[-1].start()
-    gate_up(right)
-    down(right)
-    sends.append(net.copy(parts_out.at[right, h1], from_left.at[h1], to_right))
-    sends[-1].start()
-    gather.finish()
-    gate_up(across)
-    down(across)
-    relays = share([
-        net.copy(parts_out.at[across, h0], relay.at[0], to_right),
-        net.copy(parts_out.at[across, h1], relay.at[1], to_left),
-    ])
-    for k, (peer, rows, dst, to) in enumerate(((right, h0, from_left, to_right), (left, h1, from_right, to_left))):
-        relays[k].wait_recv()
-        relay_sum[k] = (parts_out[peer, rows, :].astype(F32) + relay[k].astype(F32)).astype(BF16)
-        sends.append(net.copy(relay_sum.at[k], dst.at[rows], to))
-        sends[-1].start()
-    for copy in relays:
-        copy.wait_send()
-    for copy in sends:
+    relays, sends = [None] * STEPS, [None] * STEPS
+
+    def halves(s):
+        return pl.ds(s * PART, PART // 2), pl.ds(s * PART + PART // 2, PART // 2)
+
+    def send_parts(s):
+        h0, h1 = halves(s)
+        kept = pl.ds(s * (PART // 2), PART // 2)
+        relays[s] = share([
+            net.copy(parts_out.at[across, h0], relay.at[0, kept], to_right),
+            net.copy(parts_out.at[across, h1], relay.at[1, kept], to_left),
+        ])
+        sends[s] = share([
+            net.copy(parts_out.at[left, h0], from_right.at[h0], to_left),
+            net.copy(parts_out.at[right, h1], from_left.at[h1], to_right),
+        ])
+
+    def send_sums(s):
+        h0, h1 = halves(s)
+        kept = pl.ds(s * (PART // 2), PART // 2)
+        for k, (peer, rows, dst, to) in enumerate(((right, h0, from_left, to_right), (left, h1, from_right, to_left))):
+            relays[s][k].wait_recv()
+            relay_sum[k, kept] = (parts_out[peer, rows, :].astype(F32) + relay[k, kept].astype(F32)).astype(BF16)
+            sends[s] += share([net.copy(relay_sum.at[k, kept], dst.at[rows], to)])
+
+    def last(s):
+        for copy in relays[s]:
+            copy.wait_send()
+        for copy in sends[s]:
+            copy.wait()
+
+        def rows_of(r, _):
+            rows = pl.ds(pl.multiple_of(s * PART + r * 32, 32), 32)
+            v = parts_out[x, rows, :].astype(F32) + from_left[rows, :].astype(F32) + from_right[rows, :].astype(F32)
+            v = v * lax.rsqrt(jnp.mean(v * v, axis=1, keepdims=True) + EPS)
+            out[rows, :] = (mixed[rows, :] + 0.5 * v * params[2:3, :]).astype(BF16)
+            return 0
+
+        lax.fori_loop(0, PART // 32, rows_of, 0)
+
+    finish_step(0)
+    gathers[0].start()
+    finish_step(1)
+    gathers[1].start()
+    finish_step(2)
+    finish_step(3)
+    forward_weights(0)
+    gathers[0].forward()
+    gathers[2].start()
+    proj.finish()
+    shared_proj += share([net.copy(proj_view(across), proj_view(across), sibling)])
+    gathers[1].forward()
+    gathers[3].start()
+    forward_weights(1)
+    for copy in shared_proj:
         copy.wait()
-
-    def last(r, _):
-        rows = pl.ds(pl.multiple_of(r * 32, 32), 32)
-        v = parts_out[x, rows, :].astype(F32) + from_left[rows, :].astype(F32) + from_right[rows, :].astype(F32)
-        v = v * lax.rsqrt(jnp.mean(v * v, axis=1, keepdims=True) + EPS)
-        out[rows, :] = (mixed[rows, :] + 0.5 * v * params[2:3, :]).astype(BF16)
-        return 0
-
-    lax.fori_loop(0, OWN // 32, last, 0)
-
-
-COPIES = 120
+    for s in range(STEPS):
+        gathers[s].neighbours()
+        gathers[s].finish()
+        project(s)
+        if s == 0:
+            gathers[2].forward()
+            wait_weights(0)
+        gate_up()
+        if s == 0:
+            gathers[3].forward()
+            wait_weights(1)
+        else:
+            send_sums(s - 1)
+        down(s)
+        send_parts(s)
+    for s in range(STEPS - 1):
+        last(s)
+    send_sums(STEPS - 1)
+    last(STEPS - 1)
+
+
+COPIES = 160
 
 
 def layer(*operands):
@@ -549,9 +584,9 @@
         layer_kernel,
         name="layer",
         out_shape=jax.ShapeDtypeStruct((OWN, 2048), BF16),
-        in_specs=[hbm] * 12 + [vm] * 2 + [sm] * 2,
+        in_specs=[hbm] * 12 + [vm] * 3 + [sm] * 2,
         out_specs=vm,
-        scratch_shapes=[chan] * 10 + [
+        scratch_shapes=[chan] * 6 + [
             pltpu.VMEM((8, ROWS), F32), pltpu.VMEM((8, ROWS), F32),
             pltpu.VMEM((ROWS, 128), F32), pltpu.VMEM((ROWS, 128), F32),
             pltpu.VMEM((NBLK, 128, 512), F32), pltpu.VMEM((NBLK, 8, 512), F32),
@@ -564,10 +599,10 @@
             pltpu.VMEM((64, 512), BF16), pltpu.VMEM((8, 512), F32),
             pltpu.VMEM((3, 64, 512), BF16), pltpu.VMEM((3, 8, 512), F32),
             pltpu.VMEM((64, 512), F32), pltpu.VMEM((128, 512), F32),
-            pltpu.VMEM((ROWS, 512), BF16), pltpu.VMEM((4, OWN, 512), BF16),
+            pltpu.VMEM((4, STEPS, OWN, 512), BF16),
             pltpu.VMEM((4, 4, 2, 64, 3 * FF_DEV), BF16), pltpu.VMEM((4, 512, 2048), BF16),
-            pltpu.VMEM((OWN, 2048), BF16), pltpu.VMEM((OWN, 2048), F32),
-            pltpu.VMEM((4, OWN, 2048), BF16), pltpu.VMEM((OWN, FF_DEV), BF16),
+            pltpu.VMEM((ROWS, 2048), BF16), pltpu.VMEM((OWN, 2048), F32), pltpu.VMEM((OWN, 2048), F32),
+            pltpu.VMEM((OWN, 2048), BF16), pltpu.VMEM((OWN, FF_DEV), BF16),
             pltpu.VMEM((4, OWN, 2048), BF16),
             pltpu.VMEM((2, 128, 2048), BF16), pltpu.VMEM((2, 128, 2048), BF16),
             pltpu.VMEM((OWN, 2048), BF16), pltpu.VMEM((OWN, 2048), BF16),
@@ -586,20 +621,19 @@
     small_gain, large_gain, small_out, large_out, mixer_gain, ffn_in_gain,
     gate_proj, up_proj, down_proj, ffn_out_gain,
 ):
-    taps = jnp.concatenate([small_taps, large_taps, key_taps.reshape(4, 256), query_taps.reshape(4, 256)], axis=1)
-    head_gain = jnp.concatenate([small_gain, large_gain]).reshape(1, 512)
-    params = jnp.concatenate(
-        [
-            jnp.stack([mixer_gain, ffn_in_gain, ffn_out_gain]),
-            jnp.pad(taps, ((0, 0), (0, 1024))),
-            jnp.pad(head_gain, ((0, 0), (0, 1536))),
-        ]
-    ).astype(F32)
-    steps = jnp.concatenate([small_step.T, large_step.T, jnp.zeros((2, ROWS), F32)])
+    def placed(array, row, lane):
+        array = array.astype(F32)
+        return jnp.pad(array, ((row, 8 - row - array.shape[0]), (lane, 2048 - lane - array.shape[1])))
+
+    params = placed(mixer_gain[None], 0, 0) + placed(ffn_in_gain[None], 1, 0) + placed(ffn_out_gain[None], 2, 0)
+    taps = (small_taps, large_taps, key_taps.reshape(4, 256), query_taps.reshape(4, 256))
+    for i, tap in enumerate(taps):
+        params = params + placed(tap, 3, 256 * i)
+    params = params + placed(small_gain[None], 7, 0) + placed(large_gain[None], 7, 256)
     return layer(
         residual, small_heads, large_heads, state_keys.reshape(ROWS, 256), state_queries.reshape(ROWS, 256),
         small_gate, large_gate, gate_proj, up_proj, down_proj, small_out, large_out,
-        steps, params, small_decay, large_decay,
+        small_step.T, large_step.T, params, small_decay, large_decay,
     )
 
 

time: 160 us -> 152 us (0.950)
  Pallas kernels: 148 us -> 142 us
  other arithmetic: 3.41 us -> 1.35 us
    pallas_call x1, Pallas kernels: 148 us -> 142 us  [layer(): pl.pallas_call(layer_kernel, name='layer', out_shape=jax.ShapeDtypeStruct...]
    convert_element_type x0 -> x6, local copies, waits for them, and re-layouts: none -> 4.09 us  [placed(): array = array.astype(F32)]
    concatenate x3 -> x0, other arithmetic: 2.79 us -> none  [the longest x1 1.41 us: local(): jnp.concatenate([small_step.T, large_step.T, jnp.zeros((2, ROWS), F32)])]
    another operation x3 -> x0, local copies, waits for them, and re-layouts: 2.08 us -> none  [local(): jnp.stack([mixer_gain, ffn_in_gain, ffn_out_gain])]
where the time goes in v3:
time: 152 us
  Pallas kernels  142 us (93%)
  local copies, waits for them, and re-layouts  8.74 us (6%)
    pallas_call x1, Pallas kernels, layer(): pl.pallas_call(layer_kernel, name='layer', out_shape=jax.ShapeDtypeStruct...  142 us
    convert_element_type x6, local copies, waits for them, and re-layouts, placed(): array = array.astype(F32)  4.09 us

profile of v3, /device:TPU:1, one launch (start us, length us, event | category | flops | bytes accessed | tf_op | source)
XLA Modules:
  0.0 151.7 jit_solution(8490851111811432828)
XLA Ops:
  0.0 0.7 convert_element_type.53
  0.7 0.7 convert_element_type.54
  1.3 0.7 copy_bitcast_fusion.2
  2.0 0.7 convert_element_type.48
  2.7 0.7 convert_element_type.49
  3.4 0.7 convert_element_type.50
  4.1 1.4 convert_add_fusion.params
  5.4 2.3 %copy_bitcast_fusion = (bf16[1024,256]{1,0:T(8,128)(2,1)}, bf16[1024,256]{1,0:T(8,128)(2,1)}) fusion(bf16[128,8,2,128]{3,2,1,0:T(2,128)(2,1)} %bitcast.14, bf16[128,8,2,128]{3,2,1,0:T(2,128)(2,1)} %bitcast.15), kind=kLoop, calls=%fused_computation | loop fusion | bytes 2097152 | tf_op jit(solution)/shard_map/reshape | solution.py:634
  7.8 141.6 %layer.1 = bf16[256,2048]{1,0:T(8,128)(2,1)} custom-call(bf16[1024,2048]{1,0:T(8,128)(2,1)} %residual.1, bf16[1024,256]{1,0:T(8,128)(2,1)} %sh_in.1, bf16[1024,256]{1,0:T(8,128)(2,1)} %lh_in.1, bf16[1024,256]{1,0:T(8,128)(2,1)} %get-tuple-element.8.ks_in, bf16[1024,256]{1,0:T(8,128)(2,1)} %get-tuple-element.7.qs_in, bf16[1024,256]{1,0:T(8,128)(2,1)} %sg_in.1, ...), custom_call_target="tpu_custom_call" | custom-call | flops 22000001024 | bytes 30000000 | tf_op jit(solution)/shard_map/layer/pallas_call | solution.py:583
  149.4 2.3 %copy.35 = bf16[256,2048]{1,0:T(8,128)(2,1)} copy(bf16[256,2048]{1,0:T(8,128)(2,1)} %layer.1) | data formatting | bytes 2097152

commit v4 on v3

--- a/solution.py
+++ b/solution.py
@@ -103,13 +103,13 @@
 
 def layer_kernel(
     residual, sh_in, lh_in, ks_in, qs_in, sg_in, lg_in, gate_in, up_in, down_in, so_in, lo_in,
-    small_steps, large_steps, params, sdec, ldec,
+    small_steps, large_steps, mixer_gain, ffn_in_gain, ffn_out_gain, sgain, lgain, stap, ltap, ktap, qtap, sdec, ldec,
     out,
     xs, xl, kc, qc, sg, lg,
     dtt, ct, ccol, dcol, hloc, eoff, inside,
     halo, mine, mine_tot, sbuf, sib, sib_tot, ysend, ytot_send, yrec, ytot, zsend, ztot_send, zrec, ztot, esend, ebuf,
     chans, weights, projs, res, mix, mixed, rows_in, hidden, parts_out, relay, relay_sum, from_left, from_right,
-    send_sems, recv_sems, load_sems,
+    params, send_sems, recv_sems, load_sems,
 ):
     z = lax.axis_index("sp_0")
     y = lax.axis_index("sp_1")
@@ -187,6 +187,17 @@
     for ring in first_rings + [proj]:
         ring.start()
 
+    for i, gain in enumerate((mixer_gain, ffn_in_gain, ffn_out_gain)):
+        params[i : i + 1, :] = gain[...].astype(F32).reshape(1, 2048)
+    for i, gain in enumerate((sgain, lgain)):
+        params[7:8, i * 256 : i * 256 + 256] = gain[...].astype(F32).reshape(1, 256)
+    for i, tap in enumerate((stap, ltap)):
+        params[3:7, i * 256 : i * 256 + 256] = tap[...].astype(F32)
+    for i, tap in enumerate((ktap, qtap)):
+        for g in (0, 1):
+            at = 512 + i * 256 + g * 128
+            params[3:7, at : at + 128] = tap[:, g, :].astype(F32)
+
     dtt[...] = jnp.zeros_like(dtt)
     dtt[0:4, :] = jax.nn.softplus(small_steps[...])
     dtt[4:6, :] = jax.nn.softplus(large_steps[...])
@@ -211,7 +222,7 @@
         dcol[rows, :] = jnp.concatenate([dtt[:, rows], pad], axis=0).T
         return 0
 
-    lax.fori_loop(0, NBLK, sums, 0)
+    lax.fori_loop(0, NBLK, sums, 0, unroll=True)
 
     taps = [params[3:7, i * 256 : i * 256 + 256] for i in range(4)]
     keep = jnp.where(sp == 0, 0.0, 1.0)
@@ -269,7 +280,7 @@
         mine_tot[...] = tot + step
         return 0
 
-    lax.fori_loop(0, NBLK, states, 0)
+    lax.fori_loop(0, NBLK, states, 0, unroll=2)
 
     sbuf[...] = mine[...].astype(BF16)
     r1 = [net.copy(sbuf, sib, sibling), net.copy(mine_tot, sib_tot, sibling)]
@@ -423,7 +434,7 @@
     ]
 
     def finish_step(s):
-        lax.fori_loop(0, 4, lambda j, _: finish(s, j), 0)
+        lax.fori_loop(0, 4, lambda j, _: finish(s, j), 0, unroll=True)
 
     def share_arrived(k, which):
         zr, yr = second_rings[2 * k], second_rings[2 * k + 1]
@@ -455,7 +466,7 @@
             mix[:, cols] = acc
             return 0
 
-        lax.fori_loop(0, 8, tile, 0)
+        lax.fori_loop(0, 8, tile, 0, unroll=True)
 
         def norms(r, _):
             rows = pl.ds(pl.multiple_of(r * 32, 32), 32)
@@ -468,7 +479,7 @@
             rows_in[rows, :] = (v * params[1:2, :]).astype(BF16)
             return 0
 
-        lax.fori_loop(0, OWN // 32, norms, 0)
+        lax.fori_loop(0, OWN // 32, norms, 0, unroll=4)
         mixed[s * PART : s * PART + PART, :] = mix[pl.ds(pl.multiple_of(x * PART, PART), PART), :]
 
     def gate_up():
@@ -482,7 +493,7 @@
             hidden[:, g_cols] = (silu(both[:, :128]) * both[:, 128:]).astype(BF16)
             return 0
 
-        lax.fori_loop(0, FF_DEV // 128, tile, 0)
+        lax.fori_loop(0, FF_DEV // 128, tile, 0, unroll=True)
 
     def down(s):
         def tile(n, _):
@@ -491,7 +502,7 @@
             parts_out[:, s * PART : s * PART + PART, pl.ds(pl.multiple_of(n * 256, 256), 256)] = part
             return 0
 
-        lax.fori_loop(0, 8, tile, 0)
+        lax.fori_loop(0, 8, tile, 0, unroll=True)
 
     to_left, to_right = {"tp": left}, {"tp": right}
     relays, sends = [None] * STEPS, [None] * STEPS
@@ -541,13 +552,13 @@
     finish_step(2)
     finish_step(3)
     forward_weights(0)
+    proj.finish()
+    shared_proj += share([net.copy(proj_view(across), proj_view(across), sibling)])
     gathers[0].forward()
     gathers[2].start()
-    proj.finish()
-    shared_proj += share([net.copy(proj_view(across), proj_view(across), sibling)])
+    forward_weights(1)
     gathers[1].forward()
     gathers[3].start()
-    forward_weights(1)
     for copy in shared_proj:
         copy.wait()
     for s in range(STEPS):
@@ -584,7 +595,7 @@
         layer_kernel,
         name="layer",
         out_shape=jax.ShapeDtypeStruct((OWN, 2048), BF16),
-        in_specs=[hbm] * 12 + [vm] * 3 + [sm] * 2,
+        in_specs=[hbm] * 12 + [vm] * 11 + [sm] * 2,
         out_specs=vm,
         scratch_shapes=[chan] * 6 + [
             pltpu.VMEM((8, ROWS), F32), pltpu.VMEM((8, ROWS), F32),
@@ -606,6 +617,7 @@
             pltpu.VMEM((4, OWN, 2048), BF16),
             pltpu.VMEM((2, 128, 2048), BF16), pltpu.VMEM((2, 128, 2048), BF16),
             pltpu.VMEM((OWN, 2048), BF16), pltpu.VMEM((OWN, 2048), BF16),
+            pltpu.VMEM((8, 2048), F32),
             dma((COPIES,)), dma((COPIES,)), dma((12,)),
         ],
         compiler_params=pltpu.CompilerParams(
@@ -621,19 +633,11 @@
     small_gain, large_gain, small_out, large_out, mixer_gain, ffn_in_gain,
     gate_proj, up_proj, down_proj, ffn_out_gain,
 ):
-    def placed(array, row, lane):
-        array = array.astype(F32)
-        return jnp.pad(array, ((row, 8 - row - array.shape[0]), (lane, 2048 - lane - array.shape[1])))
-
-    params = placed(mixer_gain[None], 0, 0) + placed(ffn_in_gain[None], 1, 0) + placed(ffn_out_gain[None], 2, 0)
-    taps = (small_taps, large_taps, key_taps.reshape(4, 256), query_taps.reshape(4, 256))
-    for i, tap in enumerate(taps):
-        params = params + placed(tap, 3, 256 * i)
-    params = params + placed(small_gain[None], 7, 0) + placed(large_gain[None], 7, 256)
     return layer(
         residual, small_heads, large_heads, state_keys.reshape(ROWS, 256), state_queries.reshape(ROWS, 256),
         small_gate, large_gate, gate_proj, up_proj, down_proj, small_out, large_out,
-        small_step.T, large_step.T, params, small_decay, large_decay,
+        small_step.T, large_step.T, mixer_gain, ffn_in_gain, ffn_out_gain, small_gain, large_gain,
+        small_taps, large_taps, key_taps, query_taps, small_decay, large_decay,
     )
 
 

time: 152 us -> 128 us (0.84)
  Pallas kernels: 142 us -> 123 us
  local copies, waits for them, and re-layouts: 8.74 us -> 4.65 us
    pallas_call x1, Pallas kernels: 142 us -> 123 us  [layer(): pl.pallas_call(layer_kernel, name='layer', out_shape=jax.ShapeDtypeStruct...]
    convert_element_type x6 -> x0, local copies, waits for them, and re-layouts: 4.09 us -> none  [placed(): array = array.astype(F32)]
where the time goes in v4:
time: 128 us
  Pallas kernels  123 us (96%)
  local copies, waits for them, and re-layouts  4.65 us (4%)
    pallas_call x1, Pallas kernels, layer(): pl.pallas_call(layer_kernel, name='layer', out_shape=jax.ShapeDtypeStruct...  123 us

profile of v4, /device:TPU:1, one launch (start us, length us, event | category | flops | bytes accessed | tf_op | source)
XLA Modules:
  0.0 127.5 jit_solution(5501339653447228991)
XLA Ops:
  0.0 2.3 %copy_bitcast_fusion = (bf16[1024,256]{1,0:T(8,128)(2,1)}, bf16[1024,256]{1,0:T(8,128)(2,1)}) fusion(bf16[128,8,2,128]{3,2,1,0:T(2,128)(2,1)} %bitcast.8, bf16[128,8,2,128]{3,2,1,0:T(2,128)(2,1)} %bitcast.9), kind=kLoop, calls=%fused_computation | loop fusion | bytes 2097152 | tf_op jit(solution)/shard_map/reshape | solution.py:637
  2.3 122.9 %layer.1 = bf16[256,2048]{1,0:T(8,128)(2,1)} custom-call(bf16[1024,2048]{1,0:T(8,128)(2,1)} %residual.1, bf16[1024,256]{1,0:T(8,128)(2,1)} %sh_in.1, bf16[1024,256]{1,0:T(8,128)(2,1)} %lh_in.1, bf16[1024,256]{1,0:T(8,128)(2,1)} %get-tuple-element.6.ks_in, bf16[1024,256]{1,0:T(8,128)(2,1)} %get-tuple-element.5.qs_in, bf16[1024,256]{1,0:T(8,128)(2,1)} %sg_in.1, ...), custom_call_target="tpu_custom_call" | custom-call | flops 22000001024 | bytes 30000000 | tf_op jit(solution)/shard_map/layer/pallas_call | solution.py:594
  125.2 2.3 %copy.31 = bf16[256,2048]{1,0:T(8,128)(2,1)} copy(bf16[256,2048]{1,0:T(8,128)(2,1)} %layer.1) | data formatting | bytes 2097152

commit v5 on v4

--- a/solution.py
+++ b/solution.py
@@ -41,6 +41,10 @@
     )
 
 
+def spread_all(m):
+    return jnp.concatenate(spread(m), axis=1)
+
+
 def block_rows(b):
     return pl.ds(pl.multiple_of(b * BLOCK, BLOCK), BLOCK)
 
@@ -48,6 +52,7 @@
 OWN = 256
 STEPS = 4
 PART = OWN // STEPS
+MAIN = 192
 FF_DEV = 1408
 UP_COLS = pl.ds(0, 2 * FF_DEV)
 DOWN_COLS = pl.ds(2 * FF_DEV, FF_DEV)
@@ -173,8 +178,12 @@
         return lambda i, p=None: weights.at[span(p, 4), i, c, pl.ds(32, 32), cols]
 
     def proj_view(i, p=None):
-        size = 256 if p is None else 128
-        return projs.at[i, pl.ds(pl.multiple_of(c * 256 + (0 if p is None else p * 128), 128), size)]
+        size = MAIN if p is None else MAIN // 2
+        return projs.at[i, pl.ds(pl.multiple_of(c * 256 + (0 if p is None else p * size), 32), size)]
+
+    def slice_view(place, side, i, p=None):
+        rows = pl.ds(pl.multiple_of(c * 256 + MAIN + 16 * place, 16), 16)
+        return projs.at[i, rows, pl.ds(side * 1024, 1024) if p is None else pl.ds(side * 1024 + 512 * p, 512)]
 
     for copy in loads_own:
         copy.wait()
@@ -184,7 +193,10 @@
         for axis, at, view in (("sp_1", y, y_first), ("sp_0", z, z_first))
     ]
     proj = Ring(net, "tp", x, proj_view)
-    for ring in first_rings + [proj]:
+    cross_rings = [
+        Ring(net, "tp", x, functools.partial(slice_view, place, side)) for side, place in enumerate((y, z))
+    ]
+    for ring in first_rings + cross_rings + [proj]:
         ring.start()
 
     for i, gain in enumerate((mixer_gain, ffn_in_gain, ffn_out_gain)):
@@ -254,7 +266,7 @@
     for copy in loads_in:
         copy.wait()
     convolve((0, 1, 2))
-    for ring in first_rings:
+    for ring in first_rings + cross_rings:
         ring.forward()
 
     mine[...] = jnp.zeros_like(mine)
@@ -274,9 +286,9 @@
         state = mine[...]
         tot = mine_tot[...]
         hloc[b] = state
-        eoff[b] = jnp.exp(tot)
-        step = jnp.concatenate(spread(jnp.broadcast_to(last, (8, 128))), axis=1)
-        mine[...] = state * jnp.exp(step)[0:1, :] + jnp.concatenate([fresh_s, fresh_l], axis=1)
+        eoff[b] = jnp.exp(spread_all(tot))
+        step = jnp.broadcast_to(last, (8, 128))
+        mine[...] = state * jnp.exp(spread_all(step))[0:1, :] + jnp.concatenate([fresh_s, fresh_l], axis=1)
         mine_tot[...] = tot + step
         return 0
 
@@ -321,7 +333,7 @@
     early = jnp.where(first, my_half, sib_half)
     late = jnp.where(first, sib_half, my_half)
     t_late = jnp.where(first, t_sib, t_me)
-    chip = early * jnp.exp(t_late)[0:1, :] + late
+    chip = early * jnp.exp(spread_all(t_late))[0:1, :] + late
     chip_tot = t_me + t_sib
     ysend[...] = chip.astype(BF16)
     ytot_send[...] = chip_tot
@@ -341,46 +353,59 @@
 
     def before_of(pos, rec, tot_rec):
         e = jnp.zeros((64, 512), F32)
-        t = jnp.zeros((8, 512), F32)
+        t = jnp.zeros((8, 128), F32)
         for d in (3, 2, 1):
             valid = d <= pos
-            e = jnp.where(valid, e * jnp.exp(tot_rec[d - 1])[0:1, :] + rec[d - 1].astype(F32), e)
+            e = jnp.where(valid, e * jnp.exp(spread_all(tot_rec[d - 1]))[0:1, :] + rec[d - 1].astype(F32), e)
             t = jnp.where(valid, t + tot_rec[d - 1], t)
         return e, t
 
     ey, ty = before_of(y, yrec, ytot)
-    plane = ey * jnp.exp(chip_tot)[0:1, :] + chip
+    plane = ey * jnp.exp(spread_all(chip_tot))[0:1, :] + chip
     plane_tot = ty + chip_tot
     for e in (1, 2, 3):
         valid = y + e <= 3
-        plane = jnp.where(valid, plane * jnp.exp(ytot[3 - e])[0:1, :] + yrec[3 - e].astype(F32), plane)
+        plane = jnp.where(valid, plane * jnp.exp(spread_all(ytot[3 - e]))[0:1, :] + yrec[3 - e].astype(F32), plane)
         plane_tot = jnp.where(valid, plane_tot + ytot[3 - e], plane_tot)
     zsend[...] = plane.astype(BF16)
     ztot_send[...] = plane_tot
     r3 = peer_copies(zsend, ztot_send, zrec, ztot, zpeers)
     for copy in r3:
         copy.start()
-    for ring in first_rings:
+    for ring in first_rings + cross_rings:
         ring.finish()
+    slice_rings = [
+        Ring(net, axis, at, lambda j, p=None, i=i, side=side: slice_view(j, side, i, p))
+        for i in (left, right, across)
+        for side, (axis, at) in enumerate((("sp_1", y), ("sp_0", z)))
+    ]
+    for ring in slice_rings:
+        ring.start()
     second_rings = [
         Ring(net, axis, at, view(cols))
         for cols in (UP_COLS, DOWN_COLS)
         for axis, at, view in (("sp_0", z, z_view), ("sp_1", y, y_view))
     ]
-    for ring in second_rings:
-        ring.start()
-    shared = [
-        [net.copy(z_view(cols)(z), z_view(cols)(z), sibling), net.copy(y_view(cols)(y), y_view(cols)(y), sibling)]
-        for cols in (UP_COLS, DOWN_COLS)
-    ]
-    for group in shared:
-        for copy in group:
+    shared = [[], []]
+
+    def start_weights(k):
+        cols = (UP_COLS, DOWN_COLS)[k]
+        second_rings[2 * k].start()
+        second_rings[2 * k + 1].start()
+        shared[k] += [
+            net.copy(z_view(cols)(z), z_view(cols)(z), sibling), net.copy(y_view(cols)(y), y_view(cols)(y), sibling)
+        ]
+        for copy in shared[k]:
             copy.start()
+
+    start_weights(0)
     lax.fori_loop(4, NBLK, intra, 0)
     for copy in r3:
         copy.wait()
+    for ring in slice_rings:
+        ring.forward()
     ez, _ = before_of(z, zrec, ztot)
-    entering = ez * jnp.exp(ty)[0:1, :] + ey
+    entering = ez * jnp.exp(spread_all(ty))[0:1, :] + ey
     esend[...] = entering
     r4 = net.copy(esend, ebuf.at[half], sibling)
     r4.start()
@@ -391,7 +416,7 @@
         arrived = ebuf[i * 64 : i * 64 + 64, :]
         enter_rows.append(jnp.where(c == i, own, arrived))
     enter = jnp.concatenate(enter_rows, axis=0)
-    second = enter * jnp.exp(t_sib)[0:1, :] + sib[...].astype(F32)
+    second = enter * jnp.exp(spread_all(t_sib))[0:1, :] + sib[...].astype(F32)
     mine[...] = jnp.where(first, enter, second)
 
     proj.forward()
@@ -552,8 +577,14 @@
     finish_step(2)
     finish_step(3)
     forward_weights(0)
+    start_weights(1)
     proj.finish()
     shared_proj += share([net.copy(proj_view(across), proj_view(across), sibling)])
+    for ring in slice_rings:
+        ring.finish()
+    for i in (left, right, across):
+        here = projs.at[i, pl.ds(pl.multiple_of(c * 256 + MAIN, 32), 256 - MAIN)]
+        shared_proj += share([net.copy(here, here, sibling)])
     gathers[0].forward()
     gathers[2].start()
     forward_weights(1)
@@ -561,16 +592,22 @@
     gathers[3].start()
     for copy in shared_proj:
         copy.wait()
-    for s in range(STEPS):
+    def project_step(s):
         gathers[s].neighbours()
         gathers[s].finish()
         project(s)
+
+    project_step(0)
+    gathers[2].forward()
+    for s in range(STEPS):
         if s == 0:
-            gathers[2].forward()
             wait_weights(0)
         gate_up()
         if s == 0:
             gathers[3].forward()
+        if s + 1 < STEPS:
+            project_step(s + 1)
+        if s == 0:
             wait_weights(1)
         else:
             send_sums(s - 1)
@@ -582,7 +619,7 @@
     last(STEPS - 1)
 
 
-COPIES = 160
+COPIES = 200
 
 
 def layer(*operands):
@@ -603,12 +640,12 @@
             pltpu.VMEM((NBLK, 128, 512), F32), pltpu.VMEM((NBLK, 8, 512), F32),
             pltpu.VMEM((ROWS, 512), F32),
             pltpu.VMEM((4, 16, 256), BF16),
-            pltpu.VMEM((128, 512), F32), pltpu.VMEM((8, 512), F32),
-            pltpu.VMEM((128, 512), BF16), pltpu.VMEM((128, 512), BF16), pltpu.VMEM((8, 512), F32),
-            pltpu.VMEM((64, 512), BF16), pltpu.VMEM((8, 512), F32),
-            pltpu.VMEM((3, 64, 512), BF16), pltpu.VMEM((3, 8, 512), F32),
-            pltpu.VMEM((64, 512), BF16), pltpu.VMEM((8, 512), F32),
-            pltpu.VMEM((3, 64, 512), BF16), pltpu.VMEM((3, 8, 512), F32),
+            pltpu.VMEM((128, 512), F32), pltpu.VMEM((8, 128), F32),
+            pltpu.VMEM((128, 512), BF16), pltpu.VMEM((128, 512), BF16), pltpu.VMEM((8, 128), F32),
+            pltpu.VMEM((64, 512), BF16), pltpu.VMEM((8, 128), F32),
+            pltpu.VMEM((3, 64, 512), BF16), pltpu.VMEM((3, 8, 128), F32),
+            pltpu.VMEM((64, 512), BF16), pltpu.VMEM((8, 128), F32),
+            pltpu.VMEM((3, 64, 512), BF16), pltpu.VMEM((3, 8, 128), F32),
             pltpu.VMEM((64, 512), F32), pltpu.VMEM((128, 512), F32),
             pltpu.VMEM((4, STEPS, OWN, 512), BF16),
             pltpu.VMEM((4, 4, 2, 64, 3 * FF_DEV), BF16), pltpu.VMEM((4, 512, 2048), BF16),

time: 128 us -> 134 us (1.047)
  Pallas kernels: 123 us -> 130 us
    pallas_call x1, Pallas kernels: 123 us -> 130 us  [layer(): pl.pallas_call(layer_kernel, name='layer', out_shape=jax.ShapeDtypeStruct...]
where the time goes in v5:
time: 134 us
  Pallas kernels  130 us (97%)
  local copies, waits for them, and re-layouts  4.65 us (3%)
    pallas_call x1, Pallas kernels, layer(): pl.pallas_call(layer_kernel, name='layer', out_shape=jax.ShapeDtypeStruct...  130 us

profile of v5, /device:TPU:1, one launch (start us, length us, event | category | flops | bytes accessed | tf_op | source)
XLA Modules:
  0.0 134.2 jit_solution(15525635014666568093)
XLA Ops:
  0.0 2.3 %copy_bitcast_fusion = (bf16[1024,256]{1,0:T(8,128)(2,1)}, bf16[1024,256]{1,0:T(8,128)(2,1)}) fusion(bf16[128,8,2,128]{3,2,1,0:T(2,128)(2,1)} %bitcast.8, bf16[128,8,2,128]{3,2,1,0:T(2,128)(2,1)} %bitcast.9), kind=kLoop, calls=%fused_computation | loop fusion | bytes 2097152 | tf_op jit(solution)/shard_map/reshape | solution.py:674
  2.3 129.6 %layer.1 = bf16[256,2048]{1,0:T(8,128)(2,1)} custom-call(bf16[1024,2048]{1,0:T(8,128)(2,1)} %residual.1, bf16[1024,256]{1,0:T(8,128)(2,1)} %sh_in.1, bf16[1024,256]{1,0:T(8,128)(2,1)} %lh_in.1, bf16[1024,256]{1,0:T(8,128)(2,1)} %get-tuple-element.6.ks_in, bf16[1024,256]{1,0:T(8,128)(2,1)} %get-tuple-element.5.qs_in, bf16[1024,256]{1,0:T(8,128)(2,1)} %sg_in.1, ...), custom_call_target="tpu_custom_call" | custom-call | flops 22000001024 | bytes 30000000 | tf_op jit(solution)/shard_map/layer/pallas_call | solution.py:631
  131.9 2.3 %copy.31 = bf16[256,2048]{1,0:T(8,128)(2,1)} copy(bf16[256,2048]{1,0:T(8,128)(2,1)} %layer.1) | data formatting | bytes 2097152

commit v6 on v5

--- a/solution.py
+++ b/solution.py
@@ -192,7 +192,7 @@
         for cols in (UP_COLS, DOWN_COLS)
         for axis, at, view in (("sp_1", y, y_first), ("sp_0", z, z_first))
     ]
-    proj = Ring(net, "tp", x, proj_view)
+    proj = Ring(net, "tp", x, proj_view, (0, 1))
     cross_rings = [
         Ring(net, "tp", x, functools.partial(slice_view, place, side)) for side, place in enumerate((y, z))
     ]
@@ -382,7 +382,7 @@
     for ring in slice_rings:
         ring.start()
     second_rings = [
-        Ring(net, axis, at, view(cols))
+        Ring(net, axis, at, view(cols), (0, 1))
         for cols in (UP_COLS, DOWN_COLS)
         for axis, at, view in (("sp_0", z, z_view), ("sp_1", y, y_view))
     ]
@@ -399,6 +399,7 @@
             copy.start()
 
     start_weights(0)
+    proj.forward()
     lax.fori_loop(4, NBLK, intra, 0)
     for copy in r3:
         copy.wait()
@@ -419,10 +420,6 @@
     second = enter * jnp.exp(spread_all(t_sib))[0:1, :] + sib[...].astype(F32)
     mine[...] = jnp.where(first, enter, second)
 
-    proj.forward()
-    shared_proj = [net.copy(proj_view(i), proj_view(i), sibling) for i in (x, left, right)]
-    for copy in shared_proj:
-        copy.start()
     for copy in loads_gate:
         copy.wait()
 
@@ -474,6 +471,10 @@
     def forward_weights(k):
         second_rings[2 * k].forward()
         second_rings[2 * k + 1].forward()
+
+    def share_weights(k):
+        second_rings[2 * k].neighbours()
+        second_rings[2 * k + 1].neighbours()
         shared[k] += share_arrived(k, 0)
 
     def wait_weights(k):
@@ -578,18 +579,20 @@
     finish_step(3)
     forward_weights(0)
     start_weights(1)
+    proj.neighbours()
+    shared_proj = share([net.copy(proj_view(i), proj_view(i), sibling) for i in (left, right)])
     proj.finish()
     shared_proj += share([net.copy(proj_view(across), proj_view(across), sibling)])
+    gathers[0].forward()
+    gathers[2].start()
     for ring in slice_rings:
         ring.finish()
     for i in (left, right, across):
         here = projs.at[i, pl.ds(pl.multiple_of(c * 256 + MAIN, 32), 256 - MAIN)]
         shared_proj += share([net.copy(here, here, sibling)])
-    gathers[0].forward()
-    gathers[2].start()
-    forward_weights(1)
     gathers[1].forward()
     gathers[3].start()
+    share_weights(0)
     for copy in shared_proj:
         copy.wait()
     def project_step(s):
@@ -602,12 +605,14 @@
     for s in range(STEPS):
         if s == 0:
             wait_weights(0)
+            forward_weights(1)
+        elif s > 1:
+            project_step(s)
         gate_up()
         if s == 0:
             gathers[3].forward()
-        if s + 1 < STEPS:
-            project_step(s + 1)
-        if s == 0:
+            share_weights(1)
+            project_step(1)
             wait_weights(1)
         else:
             send_sums(s - 1)

time: 134 us -> 122 us (0.910)
  Pallas kernels: 130 us -> 117 us
    pallas_call x1, Pallas kernels: 130 us -> 117 us  [layer(): pl.pallas_call(layer_kernel, name='layer', out_shape=jax.ShapeDtypeStruct...]
where the time goes in v6:
time: 122 us; the launch traced here: 121 us
  Pallas kernels  117 us (96%)
  local copies, waits for them, and re-layouts  4.65 us (4%)
    pallas_call x1, Pallas kernels, layer(): pl.pallas_call(layer_kernel, name='layer', out_shape=jax.ShapeDtypeStruct...  117 us

profile of v6, /device:TPU:1, one launch (start us, length us, event | category | flops | bytes accessed | tf_op | source)
XLA Modules:
  0.0 121.4 jit_solution(5435135746931182302)
XLA Ops:
  0.0 2.3 %copy_bitcast_fusion = (bf16[1024,256]{1,0:T(8,128)(2,1)}, bf16[1024,256]{1,0:T(8,128)(2,1)}) fusion(bf16[128,8,2,128]{3,2,1,0:T(2,128)(2,1)} %bitcast.8, bf16[128,8,2,128]{3,2,1,0:T(2,128)(2,1)} %bitcast.9), kind=kLoop, calls=%fused_computation | loop fusion | bytes 2097152 | tf_op jit(solution)/shard_map/reshape | solution.py:679
  2.3 116.7 %layer.1 = bf16[256,2048]{1,0:T(8,128)(2,1)} custom-call(bf16[1024,2048]{1,0:T(8,128)(2,1)} %residual.1, bf16[1024,256]{1,0:T(8,128)(2,1)} %sh_in.1, bf16[1024,256]{1,0:T(8,128)(2,1)} %lh_in.1, bf16[1024,256]{1,0:T(8,128)(2,1)} %get-tuple-element.6.ks_in, bf16[1024,256]{1,0:T(8,128)(2,1)} %get-tuple-element.5.qs_in, bf16[1024,256]{1,0:T(8,128)(2,1)} %sg_in.1, ...), custom_call_target="tpu_custom_call" | custom-call | flops 22000001024 | bytes 30000000 | tf_op jit(solution)/shard_map/layer/pallas_call | solution.py:636
  119.1 2.3 %copy.31 = bf16[256,2048]{1,0:T(8,128)(2,1)} copy(bf16[256,2048]{1,0:T(8,128)(2,1)} %layer.1) | data formatting | bytes 2097152

commit v7 on v6

--- a/solution.py
+++ b/solution.py
@@ -333,45 +333,54 @@
     early = jnp.where(first, my_half, sib_half)
     late = jnp.where(first, sib_half, my_half)
     t_late = jnp.where(first, t_sib, t_me)
-    chip = early * jnp.exp(spread_all(t_late))[0:1, :] + late
     chip_tot = t_me + t_sib
-    ysend[...] = chip.astype(BF16)
     ytot_send[...] = chip_tot
-
-    def peer_copies(send, tot_send, rec, tot_rec, peers_):
-        made = []
-        for i, peer in enumerate(peers_):
-            made += [net.copy(send, rec.at[i], peer), net.copy(tot_send, tot_rec.at[i], peer)]
+    sides = (slice(0, 256), slice(256, 512))
+
+    def faded(value, tot, k):
+        return value * jnp.exp(spread_all(tot))[0:1, sides[k]]
+
+    def to_peers(send, rec, peers_):
+        made = [net.copy(send, rec(i), peer) for i, peer in enumerate(peers_)]
+        for copy in made:
+            copy.start()
         return made
 
-    r2 = peer_copies(ysend, ytot_send, yrec, ytot, ypeers)
-    for copy in r2:
-        copy.start()
+    r2, chip = [], []
+    for k in (0, 1):
+        chip.append(faded(early[:, sides[k]], t_late, k) + late[:, sides[k]])
+        ysend[k] = chip[k].astype(BF16)
+        r2.append(to_peers(ysend.at[k], lambda i, k=k: yrec.at[i, k], ypeers))
+        if k == 0:
+            r2[0] += to_peers(ytot_send, lambda i: ytot.at[i], ypeers)
     lax.fori_loop(0, 4, intra, 0)
-    for copy in r2:
-        copy.wait()
-
-    def before_of(pos, rec, tot_rec):
-        e = jnp.zeros((64, 512), F32)
-        t = jnp.zeros((8, 128), F32)
+
+    def before_of(pos, rec, tot_rec, k):
+        e = jnp.zeros((64, 256), F32)
         for d in (3, 2, 1):
-            valid = d <= pos
-            e = jnp.where(valid, e * jnp.exp(spread_all(tot_rec[d - 1]))[0:1, :] + rec[d - 1].astype(F32), e)
-            t = jnp.where(valid, t + tot_rec[d - 1], t)
-        return e, t
-
-    ey, ty = before_of(y, yrec, ytot)
-    plane = ey * jnp.exp(spread_all(chip_tot))[0:1, :] + chip
-    plane_tot = ty + chip_tot
-    for e in (1, 2, 3):
-        valid = y + e <= 3
-        plane = jnp.where(valid, plane * jnp.exp(spread_all(ytot[3 - e]))[0:1, :] + yrec[3 - e].astype(F32), plane)
-        plane_tot = jnp.where(valid, plane_tot + ytot[3 - e], plane_tot)
-    zsend[...] = plane.astype(BF16)
-    ztot_send[...] = plane_tot
-    r3 = peer_copies(zsend, ztot_send, zrec, ztot, zpeers)
-    for copy in r3:
-        copy.start()
+            e = jnp.where(d <= pos, faded(e, tot_rec[d - 1], k) + rec[d - 1, k].astype(F32), e)
+        return e
+
+    r3, ey = [], []
+    for k in (0, 1):
+        for copy in r2[k]:
+            copy.wait()
+        if k == 0:
+            ty = jnp.zeros((8, 128), F32)
+            for d in (3, 2, 1):
+                ty = jnp.where(d <= y, ty + ytot[d - 1], ty)
+            plane_tot = ty + chip_tot
+            for e in (1, 2, 3):
+                plane_tot = jnp.where(y + e <= 3, plane_tot + ytot[3 - e], plane_tot)
+            ztot_send[...] = plane_tot
+        ey.append(before_of(y, yrec, ytot, k))
+        plane = faded(ey[k], chip_tot, k) + chip[k]
+        for e in (1, 2, 3):
+            plane = jnp.where(y + e <= 3, faded(plane, ytot[3 - e], k) + yrec[3 - e, k].astype(F32), plane)
+        zsend[k] = plane.astype(BF16)
+        r3.append(to_peers(zsend.at[k], lambda i, k=k: zrec.at[i, k], zpeers))
+        if k == 0:
+            r3[0] += to_peers(ztot_send, lambda i: ztot.at[i], zpeers)
     for ring in first_rings + cross_rings:
         ring.finish()
     slice_rings = [
@@ -401,24 +410,21 @@
     start_weights(0)
     proj.forward()
     lax.fori_loop(4, NBLK, intra, 0)
-    for copy in r3:
-        copy.wait()
+    r4 = []
+    for k in (0, 1):
+        for copy in r3[k]:
+            copy.wait()
+        esend[k] = faded(before_of(z, zrec, ztot, k), ty, k) + ey[k]
+        r4.append(net.copy(esend.at[k], ebuf.at[k, half], sibling))
+        r4[k].start()
     for ring in slice_rings:
         ring.forward()
-    ez, _ = before_of(z, zrec, ztot)
-    entering = ez * jnp.exp(spread_all(ty))[0:1, :] + ey
-    esend[...] = entering
-    r4 = net.copy(esend, ebuf.at[half], sibling)
-    r4.start()
-    r4.wait()
-    own = esend[...]
-    enter_rows = []
-    for i in range(2):
-        arrived = ebuf[i * 64 : i * 64 + 64, :]
-        enter_rows.append(jnp.where(c == i, own, arrived))
-    enter = jnp.concatenate(enter_rows, axis=0)
-    second = enter * jnp.exp(spread_all(t_sib))[0:1, :] + sib[...].astype(F32)
-    mine[...] = jnp.where(first, enter, second)
+    for k in (0, 1):
+        r4[k].wait()
+        own = esend[k]
+        enter = jnp.concatenate([jnp.where(c == i, own, ebuf[k, i * 64 : i * 64 + 64, :]) for i in range(2)], axis=0)
+        second = faded(enter, t_sib, k) + sib[:, sides[k]].astype(F32)
+        mine[:, sides[k]] = jnp.where(first, enter, second)
 
     for copy in loads_gate:
         copy.wait()
@@ -521,44 +527,47 @@
 
         lax.fori_loop(0, FF_DEV // 128, tile, 0, unroll=True)
 
-    def down(s):
+    def down(s, first_tile=0, tiles=8):
         def tile(n, _):
             w = weights[n // 2, pl.ds(lax.rem(n, 2) * 2, 2), :, :, DOWN_COLS].reshape(256, FF_DEV)
             part = dot(hidden[...], w, ((1,), (1,))).astype(BF16).reshape(4, PART, 256)
             parts_out[:, s * PART : s * PART + PART, pl.ds(pl.multiple_of(n * 256, 256), 256)] = part
             return 0
 
-        lax.fori_loop(0, 8, tile, 0, unroll=True)
+        lax.fori_loop(first_tile, first_tile + tiles, tile, 0, unroll=True)
 
     to_left, to_right = {"tp": left}, {"tp": right}
-    relays, sends = [None] * STEPS, [None] * STEPS
+    relays, sends = [[] for _ in range(STEPS)], [[] for _ in range(STEPS)]
 
     def halves(s):
         return pl.ds(s * PART, PART // 2), pl.ds(s * PART + PART // 2, PART // 2)
 
-    def send_parts(s):
+    def send_parts(s, cols):
         h0, h1 = halves(s)
         kept = pl.ds(s * (PART // 2), PART // 2)
-        relays[s] = share([
-            net.copy(parts_out.at[across, h0], relay.at[0, kept], to_right),
-            net.copy(parts_out.at[across, h1], relay.at[1, kept], to_left),
-        ])
-        sends[s] = share([
-            net.copy(parts_out.at[left, h0], from_right.at[h0], to_left),
-            net.copy(parts_out.at[right, h1], from_left.at[h1], to_right),
+        relays[s] += [(cols, share([
+            net.copy(parts_out.at[across, h0, cols], relay.at[0, kept, cols], to_right),
+            net.copy(parts_out.at[across, h1, cols], relay.at[1, kept, cols], to_left),
+        ]))]
+        sends[s] += share([
+            net.copy(parts_out.at[left, h0, cols], from_right.at[h0, cols], to_left),
+            net.copy(parts_out.at[right, h1, cols], from_left.at[h1, cols], to_right),
         ])
 
     def send_sums(s):
         h0, h1 = halves(s)
         kept = pl.ds(s * (PART // 2), PART // 2)
-        for k, (peer, rows, dst, to) in enumerate(((right, h0, from_left, to_right), (left, h1, from_right, to_left))):
-            relays[s][k].wait_recv()
-            relay_sum[k, kept] = (parts_out[peer, rows, :].astype(F32) + relay[k, kept].astype(F32)).astype(BF16)
-            sends[s] += share([net.copy(relay_sum.at[k, kept], dst.at[rows], to)])
+        for cols, pair in relays[s]:
+            for k, (peer, rows, dst, to) in enumerate(((right, h0, from_left, to_right), (left, h1, from_right, to_left))):
+                pair[k].wait_recv()
+                total = parts_out[peer, rows, cols].astype(F32) + relay[k, kept, cols].astype(F32)
+                relay_sum[k, kept, cols] = total.astype(BF16)
+                sends[s] += share([net.copy(relay_sum.at[k, kept, cols], dst.at[rows, cols], to)])
 
     def last(s):
-        for copy in relays[s]:
-            copy.wait_send()
+        for _, pair in relays[s]:
+            for copy in pair:
+                copy.wait_send()
         for copy in sends[s]:
             copy.wait()
 
@@ -616,8 +625,13 @@
             wait_weights(1)
         else:
             send_sums(s - 1)
-        down(s)
-        send_parts(s)
+        if s + 1 < STEPS:
+            down(s)
+            send_parts(s, pl.ds(0, 2048))
+        else:
+            for k in (0, 1):
+                down(s, 4 * k, 4)
+                send_parts(s, pl.ds(1024 * k, 1024))
     for s in range(STEPS - 1):
         last(s)
     send_sums(STEPS - 1)
@@ -647,11 +661,11 @@
             pltpu.VMEM((4, 16, 256), BF16),
             pltpu.VMEM((128, 512), F32), pltpu.VMEM((8, 128), F32),
             pltpu.VMEM((128, 512), BF16), pltpu.VMEM((128, 512), BF16), pltpu.VMEM((8, 128), F32),
-            pltpu.VMEM((64, 512), BF16), pltpu.VMEM((8, 128), F32),
-            pltpu.VMEM((3, 64, 512), BF16), pltpu.VMEM((3, 8, 128), F32),
-            pltpu.VMEM((64, 512), BF16), pltpu.VMEM((8, 128), F32),
-            pltpu.VMEM((3, 64, 512), BF16), pltpu.VMEM((3, 8, 128), F32),
-            pltpu.VMEM((64, 512), F32), pltpu.VMEM((128, 512), F32),
+            pltpu.VMEM((2, 64, 256), BF16), pltpu.VMEM((8, 128), F32),
+            pltpu.VMEM((3, 2, 64, 256), BF16), pltpu.VMEM((3, 8, 128), F32),
+            pltpu.VMEM((2, 64, 256), BF16), pltpu.VMEM((8, 128), F32),
+            pltpu.VMEM((3, 2, 64, 256), BF16), pltpu.VMEM((3, 8, 128), F32),
+            pltpu.VMEM((2, 64, 256), F32), pltpu.VMEM((2, 128, 256), F32),
             pltpu.VMEM((4, STEPS, OWN, 512), BF16),
             pltpu.VMEM((4, 4, 2, 64, 3 * FF_DEV), BF16), pltpu.VMEM((4, 512, 2048), BF16),
             pltpu.VMEM((ROWS, 2048), BF16), pltpu.VMEM((OWN, 2048), F32), pltpu.VMEM((OWN, 2048), F32),

time: 122 us -> 122 us (level)
  no operation moved by 1% of the time
where the time goes in v7:
time: 122 us; the launch traced here: 121 us
  Pallas kernels  116 us (95%)
  local copies, waits for them, and re-layouts  4.65 us (4%)
    pallas_call x1, Pallas kernels, layer(): pl.pallas_call(layer_kernel, name='layer', out_shape=jax.ShapeDtypeStruct...  116 us

profile of v7, /device:TPU:1, one launch (start us, length us, event | category | flops | bytes accessed | tf_op | source)
XLA Modules:
  0.0 121.1 jit_solution(8602345913684394799)
XLA Ops:
  0.0 2.3 %copy_bitcast_fusion = (bf16[1024,256]{1,0:T(8,128)(2,1)}, bf16[1024,256]{1,0:T(8,128)(2,1)}) fusion(bf16[128,8,2,128]{3,2,1,0:T(2,128)(2,1)} %bitcast.8, bf16[128,8,2,128]{3,2,1,0:T(2,128)(2,1)} %bitcast.9), kind=kLoop, calls=%fused_computation | loop fusion | bytes 2097152 | tf_op jit(solution)/shard_map/reshape | solution.py:693
  2.3 116.4 %layer.1 = bf16[256,2048]{1,0:T(8,128)(2,1)} custom-call(bf16[1024,2048]{1,0:T(8,128)(2,1)} %residual.1, bf16[1024,256]{1,0:T(8,128)(2,1)} %sh_in.1, bf16[1024,256]{1,0:T(8,128)(2,1)} %lh_in.1, bf16[1024,256]{1,0:T(8,128)(2,1)} %get-tuple-element.6.ks_in, bf16[1024,256]{1,0:T(8,128)(2,1)} %get-tuple-element.5.qs_in, bf16[1024,256]{1,0:T(8,128)(2,1)} %sg_in.1, ...), custom_call_target="tpu_custom_call" | custom-call | flops 22000001024 | bytes 30000000 | tf_op jit(solution)/shard_map/layer/pallas_call | solution.py:650
  118.8 2.3 %copy.31 = bf16[256,2048]{1,0:T(8,128)(2,1)} copy(bf16[256,2048]{1,0:T(8,128)(2,1)} %layer.1) | data formatting | bytes 2097152

commit v8 on v7

--- a/solution.py
+++ b/solution.py
@@ -511,7 +511,7 @@
             rows_in[rows, :] = (v * params[1:2, :]).astype(BF16)
             return 0
 
-        lax.fori_loop(0, OWN // 32, norms, 0, unroll=4)
+        lax.fori_loop(0, OWN // 32, norms, 0, unroll=True)
         mixed[s * PART : s * PART + PART, :] = mix[pl.ds(pl.multiple_of(x * PART, PART), PART), :]
 
     def gate_up():

time: 122 us -> 119 us (0.975)
  Pallas kernels: 116 us -> 114 us
    pallas_call x1, Pallas kernels: 116 us -> 114 us  [layer(): pl.pallas_call(layer_kernel, name='layer', out_shape=jax.ShapeDtypeStruct...]
where the time goes in v8:
time: 119 us
  Pallas kernels  114 us (96%)
  local copies, waits for them, and re-layouts  4.65 us (4%)
    pallas_call x1, Pallas kernels, layer(): pl.pallas_call(layer_kernel, name='layer', out_shape=jax.ShapeDtypeStruct...  114 us

profile of v8, /device:TPU:1, one launch (start us, length us, event | category | flops | bytes accessed | tf_op | source)
XLA Modules:
  0.0 118.8 jit_solution(14390089703108185543)
XLA Ops:
  0.0 2.3 %copy_bitcast_fusion = (bf16[1024,256]{1,0:T(8,128)(2,1)}, bf16[1024,256]{1,0:T(8,128)(2,1)}) fusion(bf16[128,8,2,128]{3,2,1,0:T(2,128)(2,1)} %bitcast.8, bf16[128,8,2,128]{3,2,1,0:T(2,128)(2,1)} %bitcast.9), kind=kLoop, calls=%fused_computation | loop fusion | bytes 2097152 | tf_op jit(solution)/shard_map/reshape | solution.py:693
  2.3 114.2 %layer.1 = bf16[256,2048]{1,0:T(8,128)(2,1)} custom-call(bf16[1024,2048]{1,0:T(8,128)(2,1)} %residual.1, bf16[1024,256]{1,0:T(8,128)(2,1)} %sh_in.1, bf16[1024,256]{1,0:T(8,128)(2,1)} %lh_in.1, bf16[1024,256]{1,0:T(8,128)(2,1)} %get-tuple-element.6.ks_in, bf16[1024,256]{1,0:T(8,128)(2,1)} %get-tuple-element.5.qs_in, bf16[1024,256]{1,0:T(8,128)(2,1)} %sg_in.1, ...), custom_call_target="tpu_custom_call" | custom-call | flops 22000001024 | bytes 30000000 | tf_op jit(solution)/shard_map/layer/pallas_call | solution.py:650
  116.5 2.3 %copy.31 = bf16[256,2048]{1,0:T(8,128)(2,1)} copy(bf16[256,2048]{1,0:T(8,128)(2,1)} %layer.1) | data formatting | bytes 2097152
